TPU v7x, 512 devices: a whole 4x4x16 slice. The times are simulated.
512 devices in a mesh: fs: 128 (over z, x, core), tp: 4 (over y).
Axes of the slice: x: 4, y: 4, z: 16, core: 2. Of those that a mesh axis runs over, the one named last changes fastest.
Arguments:
- inputs: bfloat16 [16384, 2048], P('fs', 'tp'), may hold values from -24 to 24
- query_grad: bfloat16 [16384, 1024], P('fs', 'tp'), may hold values from -6 to 6
- forget_grad: bfloat16 [16384, 1024], P('fs', 'tp'), may hold values from -6 to 6
- forget_pre: bfloat16 [16384, 1024], P('fs', 'tp'), may hold values from -8 to 8
- lower_bound: float32 [1024], P('tp'), may hold values from 0.1 to 0.9
- query_weight: float32 [2048, 1024], P('fs', 'tp'), may hold values from -0.125 to 0.125
- forget_weight: float32 [2048, 1024], P('fs', 'tp'), may hold values from -0.125 to 0.125
- query_moment: float32 [2048, 1024], P('fs', 'tp'), may hold values from -6 to 6
- forget_moment: float32 [2048, 1024], P('fs', 'tp'), may hold values from -6 to 6
- query_rows: float32 [2048, 2048], P('fs'), may hold values from -0.6 to 0.6
- forget_rows: float32 [2048, 2048], P('fs'), may hold values from -0.6 to 0.6
- query_cols: float32 [8, 128, 128], P('tp'), may hold values from -0.6 to 0.6
- forget_cols: float32 [8, 128, 128], P('tp'), may hold values from -0.6 to 0.6
- query_row_root: bfloat16 [2048, 2048], P('fs'), may hold values from -2 to 2, as said below
- forget_row_root: bfloat16 [2048, 2048], P('fs'), may hold values from -2 to 2, as said below
- query_col_root: bfloat16 [8, 128, 128], P('tp'), may hold values from -2 to 2, as said below
- forget_col_root: bfloat16 [8, 128, 128], P('tp'), may hold values from -2 to 2, as said below
Outputs:
- query_master: float32 [2048, 1024], P('fs', 'tp')
- forget_master: float32 [2048, 1024], P('fs', 'tp')
- query_copy: bfloat16 [2048, 1024], P('fs', 'tp')
- forget_copy: bfloat16 [2048, 1024], P('fs', 'tp')
- query_step: float32 [2048, 1024], P('fs', 'tp')
- forget_step: float32 [2048, 1024], P('fs', 'tp')
- query_moment_next: float32 [2048, 1024], P('fs', 'tp')
- forget_moment_next: float32 [2048, 1024], P('fs', 'tp')
- query_rows_next: float32 [2048, 2048], P('fs')
- forget_rows_next: float32 [2048, 2048], P('fs')
- query_cols_next: float32 [8, 128, 128], P('tp')
- forget_cols_next: float32 [8, 128, 128], P('tp')
Inputs may be any that keep to these rules, and one draw needn't show every extreme that they name: `query_row_root`: diagonal entries 0.5 to 1.5, the others of order 2048 ** -0.5. `forget_row_root`: diagonal entries 0.5 to 1.5, the others of order 2048 ** -0.5. `query_col_root`: diagonal entries 0.5 to 1.5, the others of order 128 ** -0.5. `forget_col_root`: diagonal entries 0.5 to 1.5, the others of order 128 ** -0.5.
All inputs are finite; a program needn't handle non-finite values.
Results may differ from a plain program's by a relative error of at most 0.005.
Values may be sent and summed in bfloat16 or wider, within the bound.
A program may use at most 64 MiB of HBM per device.

v0:
```python
import jax
import jax.numpy as jnp
from jax import lax
from jax.sharding import Mesh
from jax.sharding import PartitionSpec as P

D = 2048
HW = 1024
HEAD = 128
FS = ("fs_0", "fs_1", "fs_2")


stat_decay = 0.9
moment_decay = 0.9
learn_rate = 0.02
highest = lax.Precision.HIGHEST


def from_everyone(x, axis):
    size = lax.axis_size(axis)
    return lax.all_to_all(jnp.broadcast_to(x[None], (size, *x.shape)), axis, 0, 0, tiled=True)


def in_order(tiles, dim):
    shape = list(tiles.shape[1:])
    shape[dim] *= tiles.shape[0]
    return jnp.moveaxis(tiles, 0, dim).reshape(shape)


def collect(x, axis, dim):
    tiles = from_everyone(x, axis)
    return in_order(tiles, dim)


def sum_in_order(tiles, axes, sequence):
    inside = tiles.shape[1:]
    tiles = tiles.reshape(*(lax.axis_size(a) for a in axes), *inside)
    tiles = jnp.moveaxis(tiles, sequence, range(len(axes))).reshape(-1, *inside)
    for k in sequence:
        tiles = lax.psum_scatter(tiles, axes[k], scatter_dimension=0, tiled=True)
    return tiles[0]


def cut_along(x, dim, size):
    before, after = (x.shape[:dim], x.shape[dim + 1 :])
    return jnp.moveaxis(x.reshape(*before, size, -1, *after), dim, 0)


def sum_by_axis_2(x, axes, sequence, dim):
    size = lax.axis_size(axes)
    return sum_in_order(cut_along(x, dim, size), axes, sequence)


def sent_together(arrays, axis, dim, along):
    ends, at = ([], 0)
    for a in arrays[:-1]:
        at += a.shape[along]
        ends.append(at)
    both = jnp.concatenate(arrays, axis=along)
    return tuple(jnp.split(lax.all_gather(both, axis, axis=dim, tiled=True), ends, axis=along))


def of_everyone(x, axis):
    return from_everyone(x, axis).astype(jnp.float32).sum(axis=0)


def fold_one(carry_state, shard_piece, offset, root_mine, grad_mine):
    left_sum, outer_rows, column_total = carry_state
    row_count, col_width = shard_piece.shape
    left_sum = left_sum + jnp.dot(root_mine, shard_piece, precision=highest)
    outer_piece = lax.dot_general(
        grad_mine, shard_piece, (((1,), (1,)), ((), ())), precision=highest
    )
    outer_rows = lax.dynamic_update_slice_in_dim(outer_rows, outer_piece, offset, 1)
    by_head = shard_piece.reshape(row_count, col_width // HEAD, HEAD)
    column_total = column_total + jnp.einsum("rhi,rhj->hij", by_head, by_head, precision=highest)
    return (left_sum, outer_rows, column_total)


def finish(weight, moment, rows, cols, col_root, left_sum, outer_rows, column_total, square):
    norm_scale = jnp.sqrt(D * HW / (square + 1.0))
    scale_twice = norm_scale * norm_scale
    rows_next = stat_decay * rows + (1.0 - stat_decay) / HW * scale_twice * outer_rows
    cols_next = stat_decay * cols + (1.0 - stat_decay) / D * scale_twice * column_total
    shard_rows, col_width = left_sum.shape
    shaped = left_sum.reshape(shard_rows, col_width // HEAD, HEAD)
    precond = norm_scale * jnp.einsum(
        "rhi,hij->rhj", shaped, col_root.astype(jnp.float32), precision=highest
    ).reshape(shard_rows, col_width)
    moment_next = moment_decay * moment + (1.0 - moment_decay) * precond
    update_step = moment_decay * moment_next + (1.0 - moment_decay) * precond
    master = weight - learn_rate * update_step
    return (master, master.astype(jnp.bfloat16), update_step, moment_next, rows_next, cols_next)


def on_device(
    inputs,
    query_grad,
    forget_grad,
    forget_pre,
    lower_bound,
    query_weight,
    forget_weight,
    query_moment,
    forget_moment,
    query_rows,
    forget_rows,
    query_cols,
    forget_cols,
    query_row_root,
    forget_row_root,
    query_col_root,
    forget_col_root,
):
    sigma_gate = jax.nn.sigmoid(forget_pre.astype(jnp.float32))
    forget_cot = (
        forget_grad.astype(jnp.float32) * (1.0 - lower_bound) * sigma_gate * (1.0 - sigma_gate)
    ).astype(jnp.bfloat16)
    gathered = collect(inputs, "tp", 1)
    shard_rows, col_width = query_weight.shape
    heads_here = col_width // HEAD
    row_roots = (query_row_root.astype(jnp.float32), forget_row_root.astype(jnp.float32))
    empty = (
        jnp.zeros((shard_rows, col_width), jnp.float32),
        jnp.zeros((shard_rows, D), jnp.float32),
        jnp.zeros((heads_here, HEAD, HEAD), jnp.float32),
    )
    joined = jnp.concatenate([query_grad, forget_cot], axis=1)
    summed = sum_by_axis_2(
        lax.dot_general(
            gathered, joined, (((0,), (0,)), ((), ())), preferred_element_type=jnp.float32
        ),
        FS,
        (2, 0, 1),
        0,
    )
    gradients = (summed[:, :col_width], summed[:, col_width:])
    shard_pieces = tuple(
        (
            part.astype(jnp.float32)
            for part in sent_together(
                (gradients[0].astype(jnp.bfloat16), gradients[1].astype(jnp.bfloat16)), FS, 0, 1
            )
        )
    )
    offset = jnp.int32(0)
    results = (
        fold_one(empty, shard_pieces[0], offset, row_roots[0], gradients[0]),
        fold_one(empty, shard_pieces[1], offset, row_roots[1], gradients[1]),
    )
    query_trace = jnp.sum(jnp.diagonal(results[0][2], axis1=1, axis2=2))
    forget_trace = jnp.sum(jnp.diagonal(results[1][2], axis1=1, axis2=2))
    query_outer, forget_outer, query_square, forget_square = (
        of_everyone(results[0][1].astype(jnp.bfloat16), "tp").astype(jnp.float32),
        of_everyone(results[1][1].astype(jnp.bfloat16), "tp").astype(jnp.float32),
        of_everyone(query_trace.astype(jnp.bfloat16), "tp").astype(jnp.float32),
        of_everyone(forget_trace.astype(jnp.bfloat16), "tp").astype(jnp.float32),
    )
    query_out = finish(
        query_weight,
        query_moment,
        query_rows,
        query_cols,
        query_col_root,
        results[0][0],
        query_outer,
        results[0][2],
        query_square,
    )
    forget_out = finish(
        forget_weight,
        forget_moment,
        forget_rows,
        forget_cols,
        forget_col_root,
        results[1][0],
        forget_outer,
        results[1][2],
        forget_square,
    )
    return (
        query_out[0],
        forget_out[0],
        query_out[1],
        forget_out[1],
        query_out[2],
        forget_out[2],
        query_out[3],
        forget_out[3],
        query_out[4],
        forget_out[4],
        query_out[5],
        forget_out[5],
    )


def solution(mesh):
    split = Mesh(mesh.devices.reshape(16, 4, 2, mesh.shape["tp"]), ("fs_0", "fs_1", "fs_2", "tp"))
    return jax.shard_map(
        on_device,
        mesh=split,
        in_specs=(
            P(FS, "tp"),
            P(FS, "tp"),
            P(FS, "tp"),
            P(FS, "tp"),
            P("tp"),
            P(FS, "tp"),
            P(FS, "tp"),
            P(FS, "tp"),
            P(FS, "tp"),
            P(FS, None),
            P(FS, None),
            P("tp", None, None),
            P("tp", None, None),
            P(FS, None),
            P(FS, None),
            P("tp", None, None),
            P("tp", None, None),
        ),
        out_specs=(
            P(FS, "tp"),
            P(FS, "tp"),
            P(FS, "tp"),
            P(FS, "tp"),
            P(FS, "tp"),
            P(FS, "tp"),
            P(FS, "tp"),
            P(FS, "tp"),
            P(FS, None),
            P(FS, None),
            P("tp", None, None),
            P("tp", None, None),
        ),
        check_vma=False,
    )
```

profile of v0, /device:TPU:1, one launch (start us, length us, event | category | flops | bytes accessed | tf_op | source)
XLA Modules:
  0.0 375.4 jit_solution(15456120418288334089)
XLA Ops:
  7.2 1.1 copy.76
  9.1 5.0 %all-to-all-start = ((bf16[4,128,512]{1,2,0:T(8,128)(2,1)}), bf16[4,128,512]{1,2,0:T(8,128)(2,1)S(1)}, u32[]{:S(2)}, u32[]{:S(2)}) async-start(bf16[4,128,512]{1,2,0:T(8,128)(2,1)} %broadcast_in_dim.16), calls=%async_computation | async-start | bytes 1048576 | tf_op jit(solution)/shard_map/all_to_all | solution.py:21
  15.8 5.3 %all-to-all-done = bf16[4,128,512]{1,2,0:T(8,128)(2,1)S(1)} async-done(((bf16[4,128,512]{1,2,0:T(8,128)(2,1)}), bf16[4,128,512]{1,2,0:T(8,128)(2,1)S(1)}, u32[]{:S(2)}, u32[]{:S(2)}) %all-to-all-start) | async-done | bytes 524320 | tf_op jit(solution)/shard_map/all_to_all | solution.py:21
  21.1 2.7 convolution_bitcast_fusion
  23.8 5.4 %copy.77 = f32[2048,512]{1,0:T(8,128)} copy(f32[2048,512]{0,1:T(8,128)} %convolution_bitcast_fusion) | data formatting | bytes 8388608 | tf_op jit(solution)/shard_map/dot_general | solution.py:130
  29.1 5.0 %copy.78 = f32[2,16,4,16,512]{4,3,2,1,0:T(8,128)} copy(f32[2,16,4,16,512]{4,3,0,2,1:T(8,128)} %bitcast.52) | data formatting | bytes 8388608 | tf_op jit(solution)/shard_map/transpose | solution.py:38
  34.2 28.8 %reduce-scatter.4.cloned.1.call-done = f32[64,16,512]{2,1,0:T(8,128)} async-done(((f32[128,16,512]{2,1,0:T(8,128)}), f32[64,16,512]{2,1,0:T(8,128)}) %reduce-scatter.4.cloned.1.call-update) | async-done | bytes 2097168 | tf_op jit(solution)/shard_map/reduce_scatter | solution.py:40
  63.1 66.8 %reduce-scatter.6.cloned.1.call-done = f32[4,16,512]{2,1,0:T(8,128)} async-done(((f32[64,16,512]{2,1,0:T(8,128)}), f32[4,16,512]{2,1,0:T(8,128)}) %reduce-scatter.6.cloned.1.call-update) | async-done | bytes 131088 | tf_op jit(solution)/shard_map/reduce_scatter | solution.py:40
  130.0 36.8 %reduce-scatter.8.cloned.1.call-done = f32[1,16,512]{2,1,0:T(8,128)} async-done(((f32[4,16,512]{2,1,0:T(8,128)}), f32[1,16,512]{2,1,0:T(8,128)}) %reduce-scatter.8.cloned.1.call-update) | async-done | bytes 32784 | tf_op jit(solution)/shard_map/reduce_scatter | solution.py:40
  168.2 145.5 %all-gather.2.cloned.1.call-done = bf16[2048,512]{1,0:T(8,128)(2,1)} async-done(((bf16[16,512]{1,0:T(8,128)(2,1)}), bf16[2048,512]{1,0:T(8,128)(2,1)}) %all-gather.2.cloned.1.call-update) | async-done | bytes 2097168 | tf_op jit(solution)/shard_map/all_gather | solution.py:60
  313.7 1.7 fusion.20
  317.6 4.6 %copy.81 = f32[2,128,128]{0,2,1:T(8,128)} copy(f32[2,128,128]{2,1,0:T(8,128)S(1)} %fusion.22) | data formatting | bytes 262144 | tf_op jit(solution)/shard_map/rhi,rhj->hij/dot_general | solution.py:76
  322.2 1.8 gather_fusion
  324.6 1.2 broadcast_in_dim.17
  325.8 4.0 %all-to-all-start.1 = ((bf16[4,1,1]{2,1,0:T(2,128)(2,1)}), bf16[4,1,1]{2,1,0:T(2,128)(2,1)S(1)}, u32[]{:S(2)}, u32[]{:S(2)}) async-start(bf16[4,1,1]{2,1,0:T(2,128)(2,1)} %broadcast_in_dim.17), calls=%async_computation.4 | async-start | bytes 4096 | tf_op jit(solution)/shard_map/all_to_all | solution.py:21
  329.8 4.6 %copy.87 = f32[2,128,128]{0,2,1:T(8,128)} copy(f32[2,128,128]{2,1,0:T(8,128)S(1)} %fusion.23) | data formatting | bytes 262144 | tf_op jit(solution)/shard_map/rhi,rhj->hij/dot_general | solution.py:76
  334.5 1.8 gather_fusion.1
  339.3 1.3 broadcast_in_dim.18
  340.6 4.2 %all-to-all-start.2 = ((bf16[4,1,1]{2,1,0:T(2,128)(2,1)}), bf16[4,1,1]{2,1,0:T(2,128)(2,1)S(1)}, u32[]{:S(2)}, u32[]{:S(2)}) async-start(bf16[4,1,1]{2,1,0:T(2,128)(2,1)} %broadcast_in_dim.18), calls=%async_computation.5 | async-start | bytes 4096 | tf_op jit(solution)/shard_map/all_to_all | solution.py:21
  346.3 2.6 all-to-all-done.2
  349.6 3.4 all-to-all-start.3
  356.2 2.3 all-to-all-done.3
  359.2 3.4 all-to-all-start.4
  363.4 4.8 %all-to-all-done.4 = bf16[4,16,2048]{2,1,0:T(8,128)(2,1)S(1)} async-done(((bf16[4,16,2048]{2,1,0:T(8,128)(2,1)}), bf16[4,16,2048]{2,1,0:T(8,128)(2,1)S(1)}, u32[]{:S(2)}, u32[]{:S(2)}) %all-to-all-start.4) | async-done | bytes 262176 | tf_op jit(solution)/shard_map/all_to_all | solution.py:21
  (69 shorter events, 15.8 us)
Async XLA Ops:
  7.2 331.6 %copy-start = (bf16[16,2048]{1,0:T(8,128)(2,1)S(1)}, bf16[16,2048]{1,0:T(8,128)(2,1)}, u32[]{:S(2)}) copy-start(bf16[16,2048]{1,0:T(8,128)(2,1)} %param.31) | copy-start | bytes 196612
  7.2 13.9 %copy-start.7 = (bf16[128,256]{1,0:T(8,128)(2,1)S(1)}, bf16[128,256]{1,0:T(8,128)(2,1)}, u32[]{:S(2)}) copy-start(bf16[128,256]{1,0:T(8,128)(2,1)} %param.18) | copy-start | bytes 196612
  9.1 11.9 %all-to-all-start = ((bf16[4,128,512]{1,2,0:T(8,128)(2,1)}), bf16[4,128,512]{1,2,0:T(8,128)(2,1)S(1)}, u32[]{:S(2)}, u32[]{:S(2)}) async-start(bf16[4,128,512]{1,2,0:T(8,128)(2,1)} %broadcast_in_dim.16), calls=%async_computation | async-start | bytes 1048576 | tf_op jit(solution)/shard_map/all_to_all | solution.py:21
  14.1 48.9 %reduce-scatter.4.cloned.1.call-start = ((), (), s32[]{:S(2)}) async-start(), calls=%async_computation.8 | async-start | bytes 6291456 | tf_op jit(solution)/shard_map/reduce_scatter | solution.py:40
  34.2 95.8 %reduce-scatter.6.cloned.1.call-start = ((), (), s32[]{:S(2)}) async-start(), calls=%async_computation.9 | async-start | bytes 2228224 | tf_op jit(solution)/shard_map/reduce_scatter | solution.py:40
  63.1 103.7 %reduce-scatter.8.cloned.1.call-start = ((), (), s32[]{:S(2)}) async-start(), calls=%async_computation.10 | async-start | bytes 163840 | tf_op jit(solution)/shard_map/reduce_scatter | solution.py:40
  130.0 183.7 %all-gather.2.cloned.1.call-start = ((), (), s32[]{:S(2)}) async-start(), calls=%async_computation.11 | async-start | bytes 2113536 | tf_op jit(solution)/shard_map/all_gather | solution.py:60
  325.8 13.5 %all-to-all-start.1 = ((bf16[4,1,1]{2,1,0:T(2,128)(2,1)}), bf16[4,1,1]{2,1,0:T(2,128)(2,1)S(1)}, u32[]{:S(2)}, u32[]{:S(2)}) async-start(bf16[4,1,1]{2,1,0:T(2,128)(2,1)} %broadcast_in_dim.17), calls=%async_computation.4 | async-start | bytes 4096 | tf_op jit(solution)/shard_map/all_to_all | solution.py:21
  329.8 7.0 %copy-start.1 = (bf16[2048,512]{1,0:T(8,128)(2,1)S(1)}, bf16[2048,512]{1,0:T(8,128)(2,1)}, u32[]{:S(2)}) copy-start(bf16[2048,512]{1,0:T(8,128)(2,1)} %all-gather.2.cloned.1.call-done) | copy-start | bytes 6291460
  329.8 7.0 %copy-start.6 = (f32[1,16,512]{2,1,0:T(8,128)S(1)}, f32[1,16,512]{2,1,0:T(8,128)}, u32[]{:S(2)}) copy-start(f32[1,16,512]{2,1,0:T(8,128)} %reduce-scatter.8.cloned.1.call-done) | copy-start | bytes 98308
  334.5 4.6 %copy-start.8 = (bf16[16,2048]{1,0:T(8,128)(2,1)S(1)}, bf16[16,2048]{1,0:T(8,128)(2,1)}, u32[]{:S(2)}) copy-start(bf16[16,2048]{1,0:T(8,128)(2,1)} %param.30) | copy-start | bytes 196612
  337.8 16.7 %copy-start.9 = (bf16[2,128,128]{2,1,0:T(8,128)(2,1)S(1)}, bf16[2,128,128]{2,1,0:T(8,128)(2,1)}, u32[]{:S(2)}) copy-start(bf16[2,128,128]{2,1,0:T(8,128)(2,1)} %param.32) | copy-start | bytes 196612
  337.8 16.9 %copy-start.10 = (bf16[2,128,128]{2,1,0:T(8,128)(2,1)S(1)}, bf16[2,128,128]{2,1,0:T(8,128)(2,1)}, u32[]{:S(2)}) copy-start(bf16[2,128,128]{2,1,0:T(8,128)(2,1)} %param.33) | copy-start | bytes 196612
  337.8 17.0 %copy-start.4 = (f32[2,128,128]{2,1,0:T(8,128)S(1)}, f32[2,128,128]{2,1,0:T(8,128)}, u32[]{:S(2)}) copy-start(f32[2,128,128]{2,1,0:T(8,128)} %param.29) | copy-start | bytes 393220
  337.8 17.0 %copy-start.5 = (f32[2,128,128]{2,1,0:T(8,128)S(1)}, f32[2,128,128]{2,1,0:T(8,128)}, u32[]{:S(2)}) copy-start(f32[2,128,128]{2,1,0:T(8,128)} %param.28) | copy-start | bytes 393220
  338.7 16.8 %copy-start.11 = (f32[16,256]{1,0:T(8,128)S(1)}, f32[16,256]{1,0:T(8,128)}, u32[]{:S(2)}) copy-start(f32[16,256]{1,0:T(8,128)} %param.23) | copy-start | bytes 49156
  338.8 16.8 %copy-start.12 = (f32[16,256]{1,0:T(8,128)S(1)}, f32[16,256]{1,0:T(8,128)}, u32[]{:S(2)}) copy-start(f32[16,256]{1,0:T(8,128)} %param.25) | copy-start | bytes 49156
  338.8 16.8 %copy-start.13 = (f32[16,256]{1,0:T(8,128)S(1)}, f32[16,256]{1,0:T(8,128)}, u32[]{:S(2)}) copy-start(f32[16,256]{1,0:T(8,128)} %param.22) | copy-start | bytes 49156
  338.8 16.8 %copy-start.14 = (f32[16,256]{1,0:T(8,128)S(1)}, f32[16,256]{1,0:T(8,128)}, u32[]{:S(2)}) copy-start(f32[16,256]{1,0:T(8,128)} %param.24) | copy-start | bytes 49156
  339.1 23.6 %copy-start.2 = (f32[16,2048]{1,0:T(8,128)S(1)}, f32[16,2048]{1,0:T(8,128)}, u32[]{:S(2)}) copy-start(f32[16,2048]{1,0:T(8,128)} %param.26) | copy-start | bytes 393220
  339.3 28.9 %copy-start.3 = (f32[16,2048]{1,0:T(8,128)S(1)}, f32[16,2048]{1,0:T(8,128)}, u32[]{:S(2)}) copy-start(f32[16,2048]{1,0:T(8,128)} %param.27) | copy-start | bytes 393220
  340.6 8.3 %all-to-all-start.2 = ((bf16[4,1,1]{2,1,0:T(2,128)(2,1)}), bf16[4,1,1]{2,1,0:T(2,128)(2,1)S(1)}, u32[]{:S(2)}, u32[]{:S(2)}) async-start(bf16[4,1,1]{2,1,0:T(2,128)(2,1)} %broadcast_in_dim.18), calls=%async_computation.5 | async-start | bytes 4096 | tf_op jit(solution)/shard_map/all_to_all | solution.py:21
  349.6 8.9 %all-to-all-start.3 = ((bf16[4,16,2048]{2,1,0:T(8,128)(2,1)}), bf16[4,16,2048]{2,1,0:T(8,128)(2,1)S(1)}, u32[]{:S(2)}, u32[]{:S(2)}) async-start(bf16[4,16,2048]{2,1,0:T(8,128)(2,1)} %broadcast_in_dim.19), calls=%async_computation.6 | async-start | bytes 524288 | tf_op jit(solution)/shard_map/all_to_all | solution.py:21
  359.2 8.9 %all-to-all-start.4 = ((bf16[4,16,2048]{2,1,0:T(8,128)(2,1)}), bf16[4,16,2048]{2,1,0:T(8,128)(2,1)S(1)}, u32[]{:S(2)}, u32[]{:S(2)}) async-start(bf16[4,16,2048]{2,1,0:T(8,128)(2,1)} %broadcast_in_dim.20), calls=%async_computation.7 | async-start | bytes 524288 | tf_op jit(solution)/shard_map/all_to_all | solution.py:21
Sparse Core Ops, SparseCore 0:
  34.3 28.7 reduce-scatter.3
  65.9 64.0 reduce-scatter.5
  132.8 33.9 reduce-scatter.7
  170.4 143.2 all-gather.1
where the time goes:
time: 378 us; the launch traced here: 375 us
  waiting for transfers between devices  293 us (78%)
  local copies, waits for them, and re-layouts  33 us (9%)
  starting transfers between devices  20.2 us (5%)
  between operations  15.5 us (4%)
  other arithmetic  7.48 us (2%)
  matrix products  6.23 us (2%)
    all_gather x1, waiting for transfers between devices, sent_together(): lax.all_gather(both, axis, axis=dim, tiled=True)  146 us
    reduce_scatter x3, waiting for transfers between devices, sum_in_order(): tiles = lax.psum_scatter(tiles, axes[k], scatter_dimension=0, tiled=True)  132 us
    all_to_all x5, starting transfers between devices, from_everyone(): lax.all_to_all(jnp.broadcast_to(x[None], (size, *x.shape)), axis, 0, 0, t...  20.1 us
    all_to_all x5, waiting for transfers between devices, from_everyone(): lax.all_to_all(jnp.broadcast_to(x[None], (size, *x.shape)), axis, 0, 0, t...  15 us
    dot_general x2, local copies, waits for them, and re-layouts, fold_one(): jnp.einsum('rhi,rhj->hij', by_head, by_head, precision=highest)  9.25 us
  transfers between devices with their start and end apart: 9, of which 8 were waited for; matrix products, arithmetic and copies ran while one was open for 4% of the time, Pallas kernels for 0%

commit v1 on v0

v1 whole, which is shorter than its diff:
```python
import jax
import jax.numpy as jnp
from jax import lax
from jax.experimental import pallas as pl
from jax.experimental.pallas import tpu as pltpu
from jax.sharding import Mesh
from jax.sharding import PartitionSpec as P

D = 2048
HW = 1024
HEAD = 128
FS = ("fs_0", "fs_1", "fs_2")
MESH = pl.DeviceIdType.MESH
COPIES = 96

stat_decay = 0.9
moment_decay = 0.9
learn_rate = 0.02
highest = lax.Precision.HIGHEST
f32 = jnp.float32
bf16 = jnp.bfloat16


class Net:
    def __init__(self, send, recv):
        self.send, self.recv, self.made = send, recv, []

    def copy(self, src, dst, **where):
        i = len(self.made)
        made = pltpu.make_async_remote_copy(
            src_ref=src,
            dst_ref=dst,
            send_sem=self.send.at[i],
            recv_sem=self.recv.at[i],
            device_id=where,
            device_id_type=MESH,
        )
        made.start()
        self.made.append(made)
        return made


def dot(a, b):
    return jnp.dot(a, b, preferred_element_type=f32)


def kernel(
    x_ref, qg_ref, fg_ref, fp_ref, lb_ref, rq_ref, rf_ref, cq_ref, cf_ref,
    outer_ref, pre_ref, col_ref, sq_ref,
    xy, xx, tr, gx, rall, rp, pmine, pout, pin, gp, r1, sf, sb, r2, g, o, orv, pres, cols,
    send, recv,
):
    z, x, k, y = (lax.axis_index(n) for n in ("fs_0", "fs_1", "fs_2", "tp"))
    ko = 1 - k
    at = lambda v, n, m: lax.rem(v + n + m, m)
    xp, xm, x2 = at(x, 1, 4), at(x, -1, 4), at(x, 2, 4)
    yp, ym, y2 = at(y, 1, 4), at(y, -1, 4), at(y, 2, 4)
    aw, b = z // 4, lax.rem(z, 4)
    bp, bm, b2 = at(b, 1, 4), at(b, -1, 4), at(b, 2, 4)
    zat = lambda n: at(z, n, 16)
    net = Net(send, recv)

    barrier = pltpu.get_barrier_semaphore()
    partners = [dict(fs_2=ko), dict(fs_1=xp), dict(fs_1=xm)]
    partners += [dict(tp=yy, fs_2=kk) for yy in (yp, ym) for kk in (k, ko)]
    partners += [dict(fs_0=zat(n)) for n in (1, -1, 2, -2, 4, -4, 8)]
    for who in partners:
        pl.semaphore_signal(barrier, inc=1, device_id=who, device_id_type=MESH)

    for n in range(4):
        xy[y, n] = x_ref[:, n * 128 : (n + 1) * 128].T
    gx[x, 0] = qg_ref[...]
    gate = jax.nn.sigmoid(fp_ref[...].astype(f32))
    gx[x, 1] = (fg_ref[...].astype(f32) * (1.0 - lb_ref[...]) * gate * (1.0 - gate)).astype(bf16)
    for n in range(16):
        rall[0, n] = rq_ref[:, n * 128 : (n + 1) * 128]
        rall[1, n] = rf_ref[:, n * 128 : (n + 1) * 128]
    pl.semaphore_wait(barrier, len(partners))

    lo, hi = pl.ds(0, 2), pl.ds(2, 2)
    ya_ = net.copy(xy.at[y, lo], xy.at[y, lo], tp=yp)
    yc_ = net.copy(xy.at[y, hi], xy.at[y, hi], tp=ym)
    ga_ = net.copy(gx.at[x, 0], gx.at[x, 0], fs_1=xp)
    gc_ = net.copy(gx.at[x, 1], gx.at[x, 1], fs_1=xm)
    yb_ = net.copy(xy.at[y, hi], xy.at[y, hi], tp=yp)
    yd_ = net.copy(xy.at[y, lo], xy.at[y, lo], tp=ym)
    gb_ = net.copy(gx.at[x, 1], gx.at[x, 1], fs_1=xp)
    gd_ = net.copy(gx.at[x, 0], gx.at[x, 0], fs_1=xm)
    rc_ = net.copy(rall.at[ko], rp, fs_2=ko)

    at_a = (y, ym, yp, y2)
    xs = {}

    def xsend(j):
        a = at_a[j]
        xs[j] = [
            net.copy(xy.at[a, x2], tr.at[j], fs_1=xp if j % 2 == 0 else xm),
            net.copy(xy.at[a, xp], xx.at[x, a], fs_1=xp),
            net.copy(xy.at[a, xm], xx.at[x, a], fs_1=xm),
        ]
        xx[x, a] = xy[a, x]

    def xforward(j):
        a = at_a[j]
        xs[j][0].wait_recv()
        came, to = (xm, xp) if j % 2 == 0 else (xp, xm)
        xs[j].append(net.copy(tr.at[j], xx.at[came, a], fs_1=to))

    xsend(0)
    ya_.wait_recv()
    ye_ = net.copy(xy.at[ym, lo], xy.at[ym, lo], tp=yp)
    yc_.wait_recv()
    yf_ = net.copy(xy.at[yp, hi], xy.at[yp, hi], tp=ym)
    ga_.wait_recv()
    ge_ = net.copy(gx.at[xm, 0], gx.at[xm, 0], fs_1=xp)
    gc_.wait_recv()
    gf_ = net.copy(gx.at[xp, 1], gx.at[xp, 1], fs_1=xm)
    yb_.wait_recv()
    xsend(1)
    yd_.wait_recv()
    xsend(2)
    xforward(0)
    ye_.wait_recv()
    yf_.wait_recv()
    xsend(3)
    xforward(1)
    for c in (gb_, gd_, ge_, gf_):
        c.wait_recv()

    ps, zs = {}, {}

    def product(j):
        a = at_a[j]
        for c in xs[j][1:]:
            c.wait_recv()
        lhs = jnp.concatenate([xx[n, a] for n in range(4)], axis=1)
        pout[a] = dot(lhs, gx[:, ko].reshape(512, 256))
        pmine[a] = dot(lhs, gx[:, k].reshape(512, 256)).reshape(4, 32, 256)
        ps[j] = net.copy(pout.at[a], pin.at[a], fs_2=ko)

    def near(j):
        a = at_a[j]
        ps[j].wait_recv()
        total = pmine[a] + pin[a].reshape(4, 32, 256)
        pmine[a] = total
        gp[a] = total.astype(bf16)
        zs[j] = [
            net.copy(gp.at[a, bp], r1.at[0, a], fs_0=zat(1)),
            net.copy(gp.at[a, bm], r1.at[1, a], fs_0=zat(-1)),
            net.copy(gp.at[a, b2], r1.at[2, a], fs_0=zat(2 if j % 2 == 0 else -2)),
        ]

    product(0)
    xforward(2)
    near(0)
    product(1)
    xforward(3)
    near(1)
    product(2)
    near(2)
    product(3)
    near(3)
    for j in range(4):
        a = at_a[j]
        for c in zs[j]:
            c.wait_recv()
        total = pmine[a, b]
        for n in range(3):
            total = total + r1[n, a].astype(f32)
        sf[a] = total
        sb[a] = total.astype(bf16)
    far = [net.copy(sb.at[at(aw, i, 4)], r2.at[i - 1], fs_0=zat(4 * i)) for i in (2, 1, 3)]
    for c in far:
        c.wait_recv()
    total = sf[aw]
    for n in range(3):
        total = total + r2[n].astype(f32)
    g[aw, x, b] = total.astype(bf16)

    far = [net.copy(g.at[aw, x, b], g.at[aw, x, b], fs_0=zat(4 * i)) for i in (2, 1, 3)]
    for c in far:
        c.wait_recv()
    n1 = net.copy(g.at[:, x, b], g.at[:, x, b], fs_0=zat(1))
    n2 = net.copy(g.at[:, x, b], g.at[:, x, b], fs_0=zat(-1))
    n3 = net.copy(g.at[lo, x, b], g.at[lo, x, b], fs_0=zat(2))
    n4 = net.copy(g.at[hi, x, b], g.at[hi, x, b], fs_0=zat(-2))

    at_c = (b, bm, bp, b2)
    gs = {}

    def gsend(i):
        c = at_c[i]
        gs[i] = [
            net.copy(g.at[:, x, c], g.at[:, x, c], fs_1=xp),
            net.copy(g.at[:, x, c], g.at[:, x, c], fs_1=xm),
        ]

    def gforward(i):
        c = at_c[i]
        n, came, to = (0, xm, xp) if i % 2 == 0 else (1, xp, xm)
        gs[i][n].wait_recv()
        gs[i].append(net.copy(g.at[:, came, c], g.at[:, came, c], fs_1=to))

    gsend(0)
    n1.wait_recv()
    gsend(1)
    n2.wait_recv()
    gsend(2)
    n3.wait_recv()
    n4.wait_recv()
    gsend(3)
    for i in range(4):
        gforward(i)
    for i in range(4):
        gs[i][1 if i % 2 == 0 else 0].wait_recv()
        gs[i][2].wait_recv()

    square = jnp.zeros((8, 256), f32)
    for a in range(4):
        part = g[a].reshape(512, 256).astype(f32)
        square = square + jnp.sum((part * part).reshape(64, 8, 256), axis=0)
    square = jnp.broadcast_to(jnp.sum(square, axis=(0, 1), keepdims=True), (16, 128))
    rest = square - square.astype(bf16).astype(f32)
    top = lax.broadcasted_iota(jnp.int32, (16, 128), 0) < 8
    coded = jnp.where(top, square, rest).astype(bf16)
    o[0, 16] = coded
    o[1, 16] = coded
    mine = g[aw, b, x]
    for a in range(4):
        block = lax.dot_general(
            mine, g[a].reshape(512, 256), (((1,), (1,)), ((), ())), preferred_element_type=f32
        ).astype(bf16)
        for n in range(4):
            piece = block[:, n * 128 : (n + 1) * 128]
            o[0, 4 * a + n] = piece[:16]
            o[1, 4 * a + n] = piece[16:]
    orv[k, y] = o[k]
    h0, h1 = pl.ds(0, 8), pl.ds(8, 9)
    os = {}
    for kk, half in ((k, 0), (ko, 0), (k, 1), (ko, 1)):
        same = kk is k
        for up in (True, False):
            h = h0 if (half == 0) == up else h1
            os[same, up, h is h0] = net.copy(
                o.at[kk, h], orv.at[k, y, h], tp=yp if up else ym, fs_2=kk
            )
    oc_ = net.copy(o.at[ko], orv.at[k, y], fs_2=ko)

    rc_.wait_recv()
    left = jnp.zeros((32, 256), f32)
    gram = jnp.zeros((256, 256), f32)
    for a in range(4):
        part = g[a].reshape(512, 256)
        root = jnp.concatenate(
            [
                jnp.concatenate([rall[k, 4 * a + n] for n in range(4)], axis=1),
                jnp.concatenate([rp[4 * a + n] for n in range(4)], axis=1),
            ],
            axis=0,
        )
        left = left + dot(root, part)
        gram = gram + lax.dot_general(
            part, part, (((0,), (0,)), ((), ())), preferred_element_type=f32
        )
    for h in range(2):
        lanes = slice(h * 128, (h + 1) * 128)
        cols[0, h] = gram[lanes, lanes]
        root = jnp.where(k == 0, cq_ref[h].astype(f32), cf_ref[h].astype(f32)).astype(bf16)
        value = left[:, lanes]
        high = value.astype(bf16)
        low = (value - high.astype(f32)).astype(bf16)
        pre = dot(high, root) + dot(low, root)
        pres[0, :, lanes] = pre[:16]
        pres[1, :, lanes] = pre[16:]

    fw = []
    for same in (True, False):
        m = k if same else ko
        os[same, True, True].wait_recv()
        fw.append(net.copy(orv.at[m, ym, h0], orv.at[m, ym, h0], tp=yp))
        os[same, False, False].wait_recv()
        fw.append(net.copy(orv.at[m, yp, h1], orv.at[m, yp, h1], tp=ym))
    pc_ = net.copy(pres.at[1], pre_ref.at[k], fs_2=ko)
    cc_ = net.copy(cols.at[0], col_ref.at[k], fs_2=ko)
    pre_ref[k] = pres[0]
    col_ref[k] = cols[0]
    for same in (True, False):
        os[same, True, False].wait_recv()
        os[same, False, True].wait_recv()
    for c in (*fw, oc_, pc_, cc_):
        c.wait_recv()
    for m in range(2):
        for n in range(16):
            total = orv[m, 0, n].astype(f32)
            for q in range(1, 4):
                total = total + orv[m, q, n].astype(f32)
            outer_ref[m, :, n * 128 : (n + 1) * 128] = total
        total = orv[m, 0, 16].astype(f32)
        for q in range(1, 4):
            total = total + orv[m, q, 16].astype(f32)
        sq_ref[m] = total[:8] + total[8:]
    for c in net.made:
        c.wait_send()


def exchange(inputs, qg, fg, fp, lb, rq, rf, cq, cf):
    vm = pl.BlockSpec(memory_space=pltpu.VMEM)
    s = lambda shape, kind=bf16: pltpu.VMEM(shape, kind)
    return pl.pallas_call(
        kernel,
        out_shape=(
            jax.ShapeDtypeStruct((2, 16, D), f32),
            jax.ShapeDtypeStruct((2, 16, 256), f32),
            jax.ShapeDtypeStruct((2, 2, HEAD, HEAD), f32),
            jax.ShapeDtypeStruct((2, 8, 128), f32),
        ),
        in_specs=[vm] * 9,
        out_specs=(vm,) * 4,
        scratch_shapes=[
            s((4, 4, 128, 128)),
            s((4, 4, 128, 128)),
            s((4, 128, 128)),
            s((4, 2, 128, 256)),
            s((2, 16, 16, 128)),
            s((16, 16, 128)),
            s((4, 4, 32, 256), f32),
            s((4, 128, 256), f32),
            s((4, 128, 256), f32),
            s((4, 4, 32, 256)),
            s((3, 4, 32, 256)),
            s((4, 32, 256), f32),
            s((4, 32, 256)),
            s((3, 32, 256)),
            s((4, 4, 4, 32, 256)),
            s((2, 17, 16, 128)),
            s((2, 4, 17, 16, 128)),
            s((2, 16, 256), f32),
            s((1, 2, HEAD, HEAD), f32),
            pltpu.SemaphoreType.DMA((COPIES,)),
            pltpu.SemaphoreType.DMA((COPIES,)),
        ],
        compiler_params=pltpu.CompilerParams(collective_id=0, has_side_effects=True),
        name="exchange",
    )(inputs, qg, fg, fp, lb.reshape(1, -1), rq, rf, cq, cf)


def finish(weight, moment, rows, cols, outer, pre, col, square):
    scale = jnp.sqrt(D * HW / (square + 1.0))
    twice = scale * scale
    rows_next = stat_decay * rows + (1.0 - stat_decay) / HW * twice * outer
    cols_next = stat_decay * cols + (1.0 - stat_decay) / D * twice * col
    precond = scale * pre
    moment_next = moment_decay * moment + (1.0 - moment_decay) * precond
    step = moment_decay * moment_next + (1.0 - moment_decay) * precond
    master = weight - learn_rate * step
    return (master, master.astype(bf16), step, moment_next, rows_next, cols_next)


def on_device(inputs, qg, fg, fp, lb, qw, fw, qm, fm, qr, fr, qc, fc, qrr, frr, qcr, fcr):
    outer, pre, col, square = exchange(inputs, qg, fg, fp, lb, qrr, frr, qcr, fcr)
    q = finish(qw, qm, qr, qc, outer[0], pre[0], col[0], square[0, 0, 0])
    f = finish(fw, fm, fr, fc, outer[1], pre[1], col[1], square[1, 0, 0])
    return tuple(v for pair in zip(q, f) for v in pair)


def solution(mesh):
    split = Mesh(mesh.devices.reshape(16, 4, 2, mesh.shape["tp"]), ("fs_0", "fs_1", "fs_2", "tp"))
    both, rows, cols = P(FS, "tp"), P(FS, None), P("tp", None, None)
    return jax.shard_map(
        on_device,
        mesh=split,
        in_specs=(both,) * 4 + (P("tp"),) + (both,) * 4 + (rows,) * 2 + (cols,) * 2 + (rows,) * 2 + (cols,) * 2,
        out_specs=(both,) * 8 + (rows,) * 2 + (cols,) * 2,
        check_vma=False,
    )
```

time: 378 us -> 82.7 us (0.22)
  waiting for transfers between devices: 293 us -> 0 us
  Pallas kernels: 0 us -> 75.1 us
  local copies, waits for them, and re-layouts: 33 us -> 1.26 us
  starting transfers between devices: 20.2 us -> 0 us
  between operations: 15.5 us -> 2.24 us
  matrix products: 6.23 us -> 0 us
  other arithmetic: 7.48 us -> 3.14 us
    all_gather x1 -> x0, waiting for transfers between devices: 146 us -> none  [sent_together(): lax.all_gather(both, axis, axis=dim, tiled=True)]
    reduce_scatter x3 -> x0, waiting for transfers between devices: 132 us -> none  [sum_in_order(): tiles = lax.psum_scatter(tiles, axes[k], scatter_dimension=0, tiled=True)]
    pallas_call x0 -> x1, Pallas kernels: none -> 75.1 us  [exchange(): pl.pallas_call(kernel, out_shape=(jax.ShapeDtypeStruct((2, 16, D), f32),...]
    all_to_all x5 -> x0, starting transfers between devices: 20.1 us -> none  [from_everyone(): lax.all_to_all(jnp.broadcast_to(x[None], (size, *x.shape)), axis, 0, 0, t...]
    all_to_all x5 -> x0, waiting for transfers between devices: 15 us -> none  [from_everyone(): lax.all_to_all(jnp.broadcast_to(x[None], (size, *x.shape)), axis, 0, 0, t...]
    dot_general x3 -> x0, local copies, waits for them, and re-layouts: 14.6 us -> none  [the longest x2 9.25 us: fold_one(): jnp.einsum('rhi,rhj->hij', by_head, by_head, precision=highest)]
    dot_general x9 -> x0, matrix products: 6.23 us -> none  [the longest x1 2.71 us: on_device(): lax.dot_general(gathered, joined, (((0,), (0,)), ((), ())), preferred_ele...]
    transpose x1 -> x0, local copies, waits for them, and re-layouts: 5 us -> none  [sum_in_order(): tiles = jnp.moveaxis(tiles, sequence, range(len(axes))).reshape(-1, *inside)]
  transfers between devices with their start and end apart: 9 -> 0, of which waited for: 8 -> 0; matrix products, arithmetic and copies ran while one was open for 4% -> 0% of each run, Pallas kernels for 0% -> 0%
where the time goes in v1:
time: 82.7 us; the launch traced here: 81.8 us
  Pallas kernels  75.1 us (91%)
  other arithmetic  3.14 us (4%)
  between operations  2.24 us (3%)
  local copies, waits for them, and re-layouts  1.26 us (2%)
    pallas_call x1, Pallas kernels, exchange(): pl.pallas_call(kernel, out_shape=(jax.ShapeDtypeStruct((2, 16, D), f32),...  75.1 us
    add x1, other arithmetic, finish(): rows_next = stat_decay * rows + (1.0 - stat_decay) / HW * twice * outer  1.75 us

profile of v1, /device:TPU:1, one launch (start us, length us, event | category | flops | bytes accessed | tf_op | source)
XLA Modules:
  0.0 81.8 jit_solution(789467012108413540)
XLA Ops:
  0.6 0.0 copy-start.1
  0.7 0.0 copy-start.2
  0.7 75.1 %exchange.1 = (f32[2,16,2048]{2,1,0:T(8,128)}, f32[2,16,256]{2,1,0:T(8,128)}, f32[2,2,128,128]{3,2,1,0:T(8,128)}, f32[2,8,128]{2,1,0:T(8,128)}) custom-call(bf16[128,512]{1,0:T(8,128)(2,1)} %x_ref.1, bf16[128,256]{1,0:T(8,128)(2,1)} %qg_ref.1, bf16[128,256]{1,0:T(8,128)(2,1)} %fg_ref.1, bf16[128,256]{1,0:T(8,128)(2,1)} %fp_ref.1, f32[1,256]{1,0:T(1,128)} %bitcast.21, ...), custom_call_target="tpu_custom_call" | custom-call | tf_op jit(solution)/shard_map/exchange/pallas_call | solution.py:309
  75.8 1.2 %fusion.2 = (f32[1,1,1]{2,1,0:T(1,128)}, f32[1,1,1]{2,1,0:T(1,128)}) fusion(f32[2,8,128]{2,1,0:T(8,128)} %get-tuple-element.16), kind=kLoop, calls=%fused_computation.14 | loop fusion | bytes 16 | tf_op jit(solution)/shard_map/slice | solution.py:362
  78.5 0.0 copy-done.1
  78.5 0.0 copy-done.2
  78.5 0.0 copy-start
  78.5 0.0 copy-start.3
  78.5 0.0 copy-start.4
  78.5 1.8 %bitcast_add_fusion.2 = (f32[16,2048]{1,0:T(8,128)}, f32[16,2048]{1,0:T(8,128)}) fusion(f32[2,16,2048]{2,1,0:T(8,128)} %get-tuple-element.18, f32[16,2048]{1,0:T(8,128)S(1)} %copy-done.1, f32[]{:T(128)S(6)} %mul.134, f32[]{:T(128)S(6)} %mul.128, f32[16,2048]{1,0:T(8,128)S(1)} %copy-done.2), kind=kLoop, calls=%fused_computation.2 | loop fusion | flops 196608 | bytes 786440 | tf_op jit(solution)/shard_map/add | solution.py:350
  80.3 0.0 copy-done
  80.3 0.0 copy-done.3
  80.3 0.0 copy-done.4
  80.3 0.0 copy-start.5
  80.3 0.0 copy-start.6
  80.3 0.0 copy-start.7
  80.3 0.0 copy-start.8
  80.4 0.0 copy-start.9
  80.4 0.7 bitcast_add_fusion
  81.1 0.0 copy-done.5
  81.1 0.0 copy-done.6
  81.1 0.0 copy-done.8
  81.1 0.0 copy-done.9
  81.1 0.7 fusion
  (1 shorter events, 0.0 us)
Async XLA Ops:
  0.6 77.8 %copy-start.1 = (f32[16,2048]{1,0:T(8,128)S(1)}, f32[16,2048]{1,0:T(8,128)}, u32[]{:S(2)}) copy-start(f32[16,2048]{1,0:T(8,128)} %param.27) | copy-start | bytes 393220
  0.7 77.8 %copy-start.2 = (f32[16,2048]{1,0:T(8,128)S(1)}, f32[16,2048]{1,0:T(8,128)}, u32[]{:S(2)}) copy-start(f32[16,2048]{1,0:T(8,128)} %param.26) | copy-start | bytes 393220
  78.5 1.8 %copy-start = (f32[2,2,128,128]{3,2,1,0:T(8,128)S(1)}, f32[2,2,128,128]{3,2,1,0:T(8,128)}, u32[]{:S(2)}) copy-start(f32[2,2,128,128]{3,2,1,0:T(8,128)} %get-tuple-element.19) | copy-start | bytes 786436
  78.5 1.8 %copy-start.3 = (f32[2,128,128]{2,1,0:T(8,128)S(1)}, f32[2,128,128]{2,1,0:T(8,128)}, u32[]{:S(2)}) copy-start(f32[2,128,128]{2,1,0:T(8,128)} %param.29) | copy-start | bytes 393220
  78.5 1.8 %copy-start.4 = (f32[2,128,128]{2,1,0:T(8,128)S(1)}, f32[2,128,128]{2,1,0:T(8,128)}, u32[]{:S(2)}) copy-start(f32[2,128,128]{2,1,0:T(8,128)} %param.28) | copy-start | bytes 393220
  80.3 0.8 copy-start.5
  80.3 0.8 copy-start.6
  80.3 0.8 copy-start.7
  80.3 0.8 copy-start.8
  80.4 0.8 copy-start.9

commit v2 on v1

v2 whole, which is shorter than its diff:
```python
import jax
import jax.numpy as jnp
from jax import lax
from jax.experimental import pallas as pl
from jax.experimental.pallas import tpu as pltpu
from jax.sharding import Mesh
from jax.sharding import PartitionSpec as P

D = 2048
HW = 1024
HEAD = 128
FS = ("fs_0", "fs_1", "fs_2")
MESH = pl.DeviceIdType.MESH
COPIES = 90
TILES = 827

stat_decay = 0.9
moment_decay = 0.9
learn_rate = 0.02
highest = lax.Precision.HIGHEST
f32 = jnp.float32
bf16 = jnp.bfloat16


class Net:
    def __init__(self, send, recv):
        self.send, self.recv, self.made, self.tiles = send, recv, [], 0

    def copy(self, src, dst, **where):
        made = pltpu.make_async_remote_copy(
            src_ref=src,
            dst_ref=dst,
            send_sem=self.send,
            recv_sem=self.recv.at[len(self.made)],
            device_id=where,
            device_id_type=MESH,
        )
        made.start()
        self.made.append(made)
        size = src.dtype.itemsize
        for n in src.shape:
            size *= n
        assert size % 4096 == 0
        self.tiles += size // 4096
        return made

    def drain(self, room, **where):
        assert (len(self.made), self.tiles) == (COPIES, TILES), (len(self.made), self.tiles)
        pltpu.make_async_remote_copy(
            src_ref=room,
            dst_ref=room,
            send_sem=self.send,
            recv_sem=self.recv.at[0],
            device_id=where,
            device_id_type=MESH,
        ).wait_send()


def dot(a, b):
    return jnp.dot(a, b, preferred_element_type=f32)


def kernel(
    x_hbm, qg_hbm, fg_hbm, fp_hbm, lb_hbm, rq_hbm, rf_hbm, cq_hbm, cf_hbm,
    outer_ref, pre_ref, col_ref,
    x_ref, qg_ref, fg_ref, fp_ref, lb_ref, rq_ref, rf_ref, cq_ref, cf_ref,
    xt, xx, gx, rall, rp, pmine, pout, pin, gp, r1, sf, sb, r2, g, o, orv, prer, colr, pres, cols,
    room, send, recv, loads,
):
    z, x, k, y = (lax.axis_index(n) for n in ("fs_0", "fs_1", "fs_2", "tp"))
    ko = 1 - k
    at = lambda v, n, m: lax.rem(v + n + m, m)
    xp, xm, x2 = at(x, 1, 4), at(x, -1, 4), at(x, 2, 4)
    yp, ym, y2 = at(y, 1, 4), at(y, -1, 4), at(y, 2, 4)
    aw, b = z // 4, lax.rem(z, 4)
    bp, bm, b2 = at(b, 1, 4), at(b, -1, 4), at(b, 2, 4)
    zat = lambda n: at(z, n, 16)
    net = Net(send, recv)

    barrier = pltpu.get_barrier_semaphore()
    partners = [dict(fs_2=ko), dict(fs_1=xp), dict(fs_1=xm), dict(fs_1=x2)]
    partners += [dict(tp=yy, fs_2=kk) for yy in (yp, ym, y2) for kk in (k, ko)]
    partners += [dict(fs_0=zat(n)) for n in (1, -1, 2, -2, 4, -4, 8)]
    for who in partners:
        pl.semaphore_signal(barrier, inc=1, device_id=who, device_id_type=MESH)

    pairs = (
        (x_hbm, x_ref), (qg_hbm, qg_ref), (fg_hbm, fg_ref), (fp_hbm, fp_ref), (lb_hbm, lb_ref),
        (rq_hbm, rq_ref), (rf_hbm, rf_ref), (cq_hbm, cq_ref), (cf_hbm, cf_ref),
    )
    load = [pltpu.make_async_copy(u, v, loads.at[n]) for n, (u, v) in enumerate(pairs)]
    for c in load:
        c.start()
    load[0].wait()
    for n in range(4):
        turned = x_ref[:, n * 128 : (n + 1) * 128].T
        for q in range(4):
            xt[q, n * 32 : (n + 1) * 32] = turned[q * 32 : (q + 1) * 32]
    xx[y, x] = xt[x]
    for c in load[1:5]:
        c.wait()
    gx[x, 0] = qg_ref[...]
    gate = jax.nn.sigmoid(fp_ref[...].astype(f32))
    gx[x, 1] = (fg_ref[...].astype(f32) * (1.0 - lb_ref[...]) * gate * (1.0 - gate)).astype(bf16)
    for c in load[5:]:
        c.wait()
    for n in range(16):
        rall[0, n] = rq_ref[:, n * 128 : (n + 1) * 128]
        rall[1, n] = rf_ref[:, n * 128 : (n + 1) * 128]
    pl.semaphore_wait(barrier, len(partners))

    first = k == 0
    px = (x, xm, xp, x2)
    at_a = (y, ym, yp, y2)
    ys = {}

    def ysend(p):
        ys[p] = [
            net.copy(xx.at[y, px[p]], xx.at[y, px[p]], tp=yp),
            net.copy(xx.at[y, px[p]], xx.at[y, px[p]], tp=ym),
        ]
        if p == 3:
            ys[p].append(net.copy(xx.at[y, px[p]], xx.at[y, px[p]], tp=y2))

    def yforward(p):
        n, came, to = (0, ym, yp) if p % 2 == 0 else (1, yp, ym)
        ys[p][n].wait_recv()
        ys[p].append(net.copy(xx.at[came, px[p]], xx.at[came, px[p]], tp=to))

    xc_ = net.copy(xt.at[x2], xx.at[y, x], fs_1=x2)
    xa_ = net.copy(xt.at[xp], xx.at[y, x], fs_1=xp)
    xb_ = net.copy(xt.at[xm], xx.at[y, x], fs_1=xm)
    ysend(0)
    ga_ = net.copy(gx.at[x, 0], gx.at[x, 0], fs_1=xp)
    gc_ = net.copy(gx.at[x, 1], gx.at[x, 1], fs_1=xm)
    gb_ = net.copy(gx.at[x, 1], gx.at[x, 1], fs_1=xp)
    gd_ = net.copy(gx.at[x, 0], gx.at[x, 0], fs_1=xm)
    rc_ = net.copy(rall.at[ko], rp, fs_2=ko)
    xa_.wait_recv()
    ysend(1)
    xb_.wait_recv()
    ysend(2)
    yforward(0)
    xc_.wait_recv()
    ysend(3)
    ga_.wait_recv()
    ge_ = net.copy(gx.at[xm, 0], gx.at[xm, 0], fs_1=xp)
    gc_.wait_recv()
    gf_ = net.copy(gx.at[xp, 1], gx.at[xp, 1], fs_1=xm)
    yforward(1)
    yforward(2)
    for c in (gb_, gd_, ge_, gf_):
        c.wait_recv()

    ps, zs = {}, {}

    def product(j):
        a = at_a[j]
        lhs = jnp.concatenate([xx[a, n] for n in range(4)], axis=1)
        pout[a] = dot(lhs, gx[:, ko].reshape(512, 256))
        pmine[a] = dot(lhs, gx[:, k].reshape(512, 256)).reshape(4, 32, 256)
        ps[j] = net.copy(pout.at[a], pin.at[a], fs_2=ko)

    def near(j):
        a = at_a[j]
        ps[j].wait_recv()
        total = pmine[a] + pin[a].reshape(4, 32, 256)
        pmine[a] = total
        gp[a] = total.astype(bf16)
        zs[j] = [
            net.copy(gp.at[a, bp], r1.at[0, a], fs_0=zat(1)),
            net.copy(gp.at[a, bm], r1.at[1, a], fs_0=zat(-1)),
            net.copy(gp.at[a, b2], r1.at[2, a], fs_0=zat(2 if j % 2 == 0 else -2)),
        ]

    product(0)
    for p in (1, 3):
        ys[p][0].wait_recv()
    product(1)
    near(0)
    for p in (0, 2, 3):
        ys[p][1].wait_recv()
    product(2)
    near(1)
    for p in range(4):
        ys[p][2].wait_recv()
    product(3)
    near(2)
    near(3)
    for j in range(4):
        a = at_a[j]
        for c in zs[j]:
            c.wait_recv()
        total = pmine[a, b]
        for n in range(3):
            total = total + r1[n, a].astype(f32)
        sf[a] = total
        sb[a] = total.astype(bf16)
    far = [net.copy(sb.at[at(aw, i, 4)], r2.at[i - 1], fs_0=zat(4 * i)) for i in (2, 1, 3)]
    for c in far:
        c.wait_recv()
    total = sf[aw]
    for n in range(3):
        total = total + r2[n].astype(f32)
    mine = total.astype(bf16)
    g[aw, b, x] = mine

    far = [net.copy(g.at[aw, b, x], g.at[aw, b, x], fs_0=zat(4 * i)) for i in (2, 1, 3)]
    rc_.wait_recv()
    for c in far:
        c.wait_recv()
    lo, hi = pl.ds(0, 2), pl.ds(2, 2)
    n1 = net.copy(g.at[:, b, x], g.at[:, b, x], fs_0=zat(1))
    n2 = net.copy(g.at[:, b, x], g.at[:, b, x], fs_0=zat(-1))
    n3 = net.copy(g.at[lo, b, x], g.at[lo, b, x], fs_0=zat(2))
    n4 = net.copy(g.at[hi, b, x], g.at[hi, b, x], fs_0=zat(-2))

    at_c = (b, bm, bp, b2)
    gs, os, fw = {}, {}, []
    state = dict(left=jnp.zeros((32, 256), f32), gram=jnp.zeros((256, 256), f32), square=jnp.zeros((8, 256), f32))

    def gcopy(c, n, **where):
        return net.copy(g.at[:, c, n], g.at[:, c, n], **where)

    def gsend(i):
        gs[i, "up"] = gcopy(at_c[i], x, fs_1=xp) if i != 1 else None
        gs[i, "down"] = gcopy(at_c[i], x, fs_1=xm) if i != 2 else None

    def gforward(i):
        way, came, to = ("up", xm, xp) if i % 2 == 0 else ("down", xp, xm)
        gs[i, way].wait_recv()
        gs[i, "on"] = gcopy(at_c[i], came, fs_1=to)

    def gwait(i):
        if i == 1:
            gs["z", "up"].wait_recv()
        elif i == 2:
            gs["z", "down"].wait_recv()
        elif i == 3:
            gs[i, "up"].wait_recv()
        gs[i, "on"].wait_recv()

    chunk = lambda i: pl.ds(4 * i, 4 if i < 3 else 5)
    held = lambda i: g[:, at_c[i]].reshape(512, 256)

    def outer(i):
        part = held(i)
        wide = part.astype(f32)
        state["square"] = state["square"] + jnp.sum((wide * wide).reshape(64, 8, 256), axis=0)
        block = lax.dot_general(mine, part, (((1,), (1,)), ((), ())), preferred_element_type=f32).astype(bf16)
        for a in range(4):
            piece = block[:, a * 128 : (a + 1) * 128]
            o[0, 4 * i + a] = piece[:16]
            o[1, 4 * i + a] = piece[16:]
        if i == 3:
            square = jnp.sum(state["square"], axis=(0, 1), keepdims=True)
            square = jnp.broadcast_to(square, (16, 128))
            rest = square - square.astype(bf16).astype(f32)
            top = lax.broadcasted_iota(jnp.int32, (16, 128), 0) < 8
            coded = jnp.where(top, square, rest).astype(bf16)
            o[0, 16] = coded
            o[1, 16] = coded
        h = chunk(i)
        orv[k, y, h] = o[k, h]
        for same, kk in ((True, k), (False, ko)):
            if i == 3:
                os[i, same] = net.copy(o.at[kk, h], orv.at[k, y, h], tp=y2, fs_2=kk)
            for up in (True, False) if i % 2 == 0 else (False, True):
                os[i, same, up] = net.copy(o.at[kk, h], orv.at[k, y, h], tp=yp if up else ym, fs_2=kk)
        os[i] = net.copy(o.at[ko, h], orv.at[k, y, h], fs_2=ko)

    def stats(i):
        part, c = held(i), at_c[i]
        root = jnp.concatenate(
            [
                jnp.concatenate([rall[k, 4 * a + c] for a in range(4)], axis=1),
                jnp.concatenate([rp[4 * a + c] for a in range(4)], axis=1),
            ],
            axis=0,
        )
        state["left"] = state["left"] + dot(root, part)
        state["gram"] = state["gram"] + lax.dot_general(
            part, part, (((0,), (0,)), ((), ())), preferred_element_type=f32
        )

    def oforward(i):
        up, came, to = (True, ym, yp) if i % 2 == 0 else (False, yp, ym)
        h = chunk(i)
        for same, m in ((True, k), (False, ko)):
            os[i, same, up].wait_recv()
            fw.append(net.copy(orv.at[m, came, h], orv.at[m, came, h], tp=to))

    gsend(0)
    n1.wait_recv()
    gsend(1)
    n2.wait_recv()
    gsend(2)
    gforward(0)
    gs["z", "up"] = gcopy(b, xm, fs_0=zat(1))
    gs[0, "down"].wait_recv()
    gs["z", "down"] = gcopy(b, xp, fs_0=zat(-1))
    n3.wait_recv()
    n4.wait_recv()
    gsend(3)
    gforward(1)
    gforward(2)
    gwait(0)
    outer(0)
    gforward(3)
    stats(0)
    gwait(1)
    outer(1)
    stats(1)
    gwait(2)
    outer(2)
    stats(2)
    gwait(3)
    outer(3)
    oforward(0)
    oforward(1)
    oforward(2)
    stats(3)
    left, gram = state["left"], state["gram"]
    for h in range(2):
        lanes = slice(h * 128, (h + 1) * 128)
        cols[h] = gram[lanes, lanes]
        root = jnp.where(first, cq_ref[h].astype(f32), cf_ref[h].astype(f32)).astype(bf16)
        value = left[:, lanes]
        high = value.astype(bf16)
        low = (value - high.astype(f32)).astype(bf16)
        pre = dot(high, root) + dot(low, root)
        pres[0, :, lanes] = pre[:16]
        pres[1, :, lanes] = pre[16:]
    pc_ = net.copy(pres.at[1], prer.at[k], fs_2=ko)
    cc_ = net.copy(cols, colr.at[k], fs_2=ko)
    prer[k] = pres[0]
    colr[k] = cols[...]
    for i in range(4):
        for same in (True, False):
            if i == 3:
                os[i, same, False].wait_recv()
                os[i, same].wait_recv()
            os[i, same, i % 2 == 1].wait_recv()
        os[i].wait_recv()
    for c in (pc_, cc_):
        c.wait_recv()
    for c in fw:
        c.wait_recv()
    for m in range(2):
        total = orv[m, 0, 16].astype(f32)
        for q in range(1, 4):
            total = total + orv[m, q, 16].astype(f32)
        square = total[:8] + total[8:]
        scale = jnp.sqrt(D * HW / (square + 1.0))[:1]
        twice = scale * scale
        by_row = (1.0 - stat_decay) / HW * twice
        by_col = (1.0 - stat_decay) / D * twice
        for i in range(4):
            for a in range(4):
                total = orv[m, 0, 4 * i + a].astype(f32)
                for q in range(1, 4):
                    total = total + orv[m, q, 4 * i + a].astype(f32)
                lanes = pl.ds(pl.multiple_of((4 * a + at_c[i]) * 128, 128), 128)
                outer_ref[m, :, lanes] = by_row * total
        for h in range(2):
            lanes = slice(h * 128, (h + 1) * 128)
            pre_ref[m, :, lanes] = scale * prer[m, :, lanes]
            col_ref[m, h] = by_col * colr[m, h]
    net.drain(room, fs_2=ko)


def exchange(inputs, qg, fg, fp, lb, rq, rf, cq, cf):
    vm = pl.BlockSpec(memory_space=pltpu.VMEM)
    hbm = pl.BlockSpec(memory_space=pltpu.HBM)
    s = lambda shape, kind=bf16: pltpu.VMEM(shape, kind)
    given = (inputs, qg, fg, fp, lb.reshape(1, -1), rq, rf, cq, cf)
    return pl.pallas_call(
        kernel,
        out_shape=(
            pltpu.VMEM((2, 16, D), f32),
            pltpu.VMEM((2, 16, 256), f32),
            pltpu.VMEM((2, 2, HEAD, HEAD), f32),
        ),
        in_specs=[hbm] * 9,
        out_specs=(vm,) * 3,
        scratch_shapes=[s(v.shape, v.dtype) for v in given]
        + [
            s((4, 128, 128)),
            s((4, 4, 128, 128)),
            s((4, 2, 128, 256)),
            s((2, 16, 16, 128)),
            s((16, 16, 128)),
            s((4, 4, 32, 256), f32),
            s((4, 128, 256), f32),
            s((4, 128, 256), f32),
            s((4, 4, 32, 256)),
            s((3, 4, 32, 256)),
            s((4, 32, 256), f32),
            s((4, 32, 256)),
            s((3, 32, 256)),
            s((4, 4, 4, 32, 256)),
            s((2, 17, 16, 128)),
            s((2, 4, 17, 16, 128)),
            s((2, 16, 256), f32),
            s((2, 2, HEAD, HEAD), f32),
            s((2, 16, 256), f32),
            s((2, HEAD, HEAD), f32),
            s((TILES, 16, 128)),
            pltpu.SemaphoreType.DMA,
            pltpu.SemaphoreType.DMA((COPIES,)),
            pltpu.SemaphoreType.DMA((len(given),)),
        ],
        compiler_params=pltpu.CompilerParams(collective_id=0, has_side_effects=True),
        name="exchange",
    )(*given)


def finish(weight, moment, rows, cols, outer, precond, col):
    rows_next = stat_decay * rows + outer
    cols_next = stat_decay * cols + col
    moment_next = moment_decay * moment + (1.0 - moment_decay) * precond
    step = moment_decay * moment_next + (1.0 - moment_decay) * precond
    master = weight - learn_rate * step
    return (master, master.astype(bf16), step, moment_next, rows_next, cols_next)


def on_device(inputs, qg, fg, fp, lb, qw, fw, qm, fm, qr, fr, qc, fc, qrr, frr, qcr, fcr):
    outer, pre, col = exchange(inputs, qg, fg, fp, lb, qrr, frr, qcr, fcr)
    q = finish(qw, qm, qr, qc, outer[0], pre[0], col[0])
    f = finish(fw, fm, fr, fc, outer[1], pre[1], col[1])
    return tuple(v for pair in zip(q, f) for v in pair)


def solution(mesh):
    split = Mesh(mesh.devices.reshape(16, 4, 2, mesh.shape["tp"]), ("fs_0", "fs_1", "fs_2", "tp"))
    both, rows, cols = P(FS, "tp"), P(FS, None), P("tp", None, None)
    return jax.shard_map(
        on_device,
        mesh=split,
        in_specs=(both,) * 4 + (P("tp"),) + (both,) * 4 + (rows,) * 2 + (cols,) * 2 + (rows,) * 2 + (cols,) * 2,
        out_specs=(both,) * 8 + (rows,) * 2 + (cols,) * 2,
        check_vma=False,
    )
```

time: 82.7 us -> 71.3 us (0.86)
  Pallas kernels: 75.1 us -> 67.7 us
  between operations: 2.24 us -> 0.74 us
  other arithmetic: 3.14 us -> 2.12 us
    pallas_call x1, Pallas kernels: 75.1 us -> 67.7 us  [exchange(): pl.pallas_call(kernel, out_shape=(pltpu.VMEM((2, 16, D), f32), pltpu.VMEM...]
    slice x1 -> x0, local copies, waits for them, and re-layouts: 1.2 us -> none  [on_device(): f = finish(fw, fm, fr, fc, outer[1], pre[1], col[1], square[1, 0, 0])]
    add x2, other arithmetic: 2.49 us -> 1.47 us  [the longest x1 0.73 us: finish(): cols_next = stat_decay * cols + col]
where the time goes in v2:
time: 71.3 us; the launch traced here: 71.1 us
  Pallas kernels  67.7 us (95%)
  other arithmetic  2.12 us (3%)
  between operations  0.74 us (1%)
    pallas_call x1, Pallas kernels, exchange(): pl.pallas_call(kernel, out_shape=(pltpu.VMEM((2, 16, D), f32), pltpu.VMEM...  67.7 us

profile of v2, /device:TPU:1, one launch (start us, length us, event | category | flops | bytes accessed | tf_op | source)
XLA Modules:
  0.0 71.1 jit_solution(745640756014227392)
XLA Ops:
  0.6 0.0 copy-start.4
  0.7 0.0 copy-start.5
  0.7 0.0 copy-start.6
  0.7 0.0 copy-start.7
  0.7 0.0 copy-start.1
  0.7 67.7 %exchange.1 = (f32[2,16,2048]{2,1,0:T(8,128)S(1)}, f32[2,16,256]{2,1,0:T(8,128)S(1)}, f32[2,2,128,128]{3,2,1,0:T(8,128)S(1)}) custom-call(bf16[128,512]{1,0:T(8,128)(2,1)} %x_hbm.1, bf16[128,256]{1,0:T(8,128)(2,1)} %qg_hbm.1, bf16[128,256]{1,0:T(8,128)(2,1)} %fg_hbm.1, bf16[128,256]{1,0:T(8,128)(2,1)} %fp_hbm.1, f32[1,256]{1,0:T(1,128)} %bitcast.19, ...), custom_call_target="tpu_custom_call" | custom-call | tf_op jit(solution)/shard_map/exchange/pallas_call | solution.py:377
  68.4 0.0 copy-start
  68.5 0.0 copy-done.4
  68.5 0.0 copy-done.5
  68.5 0.0 copy-done.6
  68.5 0.0 copy-done.7
  68.5 0.7 fusion
  69.1 0.0 copy-done.1
  69.1 0.2 copy-done
  69.3 0.0 copy-start.2
  69.3 0.0 copy-start.3
  69.3 0.7 %bitcast_add_fusion.2 = (f32[16,2048]{1,0:T(8,128)}, f32[16,2048]{1,0:T(8,128)}) fusion(f32[2,16,2048]{2,1,0:T(8,128)S(1)} %get-tuple-element.16, f32[16,2048]{1,0:T(8,128)S(1)} %copy-done, f32[16,2048]{1,0:T(8,128)S(1)} %copy-done.1), kind=kLoop, calls=%fused_computation.2 | loop fusion | flops 131072 | bytes 786432 | tf_op jit(solution)/shard_map/add | solution.py:419
  70.1 0.2 copy-done.2
  70.3 0.1 copy-done.3
  70.4 0.7 %bitcast_add_fusion = (f32[2,128,128]{2,1,0:T(8,128)}, f32[2,128,128]{2,1,0:T(8,128)}) fusion(f32[2,2,128,128]{3,2,1,0:T(8,128)S(1)} %get-tuple-element.17, f32[2,128,128]{2,1,0:T(8,128)S(1)} %copy-done.2, f32[2,128,128]{2,1,0:T(8,128)S(1)} %copy-done.3), kind=kLoop, calls=%fused_computation | loop fusion | flops 131072 | bytes 786432 | tf_op jit(solution)/shard_map/add | solution.py:420
Async XLA Ops:
  0.6 67.8 %copy-start.4 = (f32[16,256]{1,0:T(8,128)S(1)}, f32[16,256]{1,0:T(8,128)}, u32[]{:S(2)}) copy-start(f32[16,256]{1,0:T(8,128)} %param.23) | copy-start | bytes 49156
  0.7 67.8 %copy-start.5 = (f32[16,256]{1,0:T(8,128)S(1)}, f32[16,256]{1,0:T(8,128)}, u32[]{:S(2)}) copy-start(f32[16,256]{1,0:T(8,128)} %param.25) | copy-start | bytes 49156
  0.7 67.8 %copy-start.6 = (f32[16,256]{1,0:T(8,128)S(1)}, f32[16,256]{1,0:T(8,128)}, u32[]{:S(2)}) copy-start(f32[16,256]{1,0:T(8,128)} %param.22) | copy-start | bytes 49156
  0.7 67.8 %copy-start.7 = (f32[16,256]{1,0:T(8,128)S(1)}, f32[16,256]{1,0:T(8,128)}, u32[]{:S(2)}) copy-start(f32[16,256]{1,0:T(8,128)} %param.24) | copy-start | bytes 49156
  0.7 68.5 %copy-start.1 = (f32[16,2048]{1,0:T(8,128)S(1)}, f32[16,2048]{1,0:T(8,128)}, u32[]{:S(2)}) copy-start(f32[16,2048]{1,0:T(8,128)} %param.26) | copy-start | bytes 393220
  68.4 0.9 %copy-start = (f32[16,2048]{1,0:T(8,128)S(1)}, f32[16,2048]{1,0:T(8,128)}, u32[]{:S(2)}) copy-start(f32[16,2048]{1,0:T(8,128)} %param.27) | copy-start | bytes 393220
  69.3 0.9 %copy-start.2 = (f32[2,128,128]{2,1,0:T(8,128)S(1)}, f32[2,128,128]{2,1,0:T(8,128)}, u32[]{:S(2)}) copy-start(f32[2,128,128]{2,1,0:T(8,128)} %param.29) | copy-start | bytes 393220
  69.3 1.1 %copy-start.3 = (f32[2,128,128]{2,1,0:T(8,128)S(1)}, f32[2,128,128]{2,1,0:T(8,128)}, u32[]{:S(2)}) copy-start(f32[2,128,128]{2,1,0:T(8,128)} %param.28) | copy-start | bytes 393220

commit v3 on v2

v3 whole, which is shorter than its diff:
```python
import jax
import jax.numpy as jnp
from jax import lax
from jax.experimental import pallas as pl
from jax.experimental.pallas import tpu as pltpu
from jax.sharding import Mesh
from jax.sharding import PartitionSpec as P

D = 2048
HW = 1024
HEAD = 128
FS = ("fs_0", "fs_1", "fs_2")
MESH = pl.DeviceIdType.MESH
SEMS = 26
TILES = 746

stat_decay = 0.9
moment_decay = 0.9
learn_rate = 0.02
highest = lax.Precision.HIGHEST
f32 = jnp.float32
bf16 = jnp.bfloat16


class Net:
    def __init__(self, send, recv, room, other):
        self.send, self.recv, self.room, self.other = send, recv, room, other
        self.names, self.sent, self.waited = {}, {}, {}

    def sem(self, name):
        return self.recv.at[self.names.setdefault(name, len(self.names))]

    def copy(self, name, src, dst, count=True, **where):
        pltpu.make_async_remote_copy(
            src_ref=src,
            dst_ref=dst,
            send_sem=self.send,
            recv_sem=self.sem(name),
            device_id=where,
            device_id_type=MESH,
        ).start()
        size = src.dtype.itemsize
        for n in src.shape:
            size *= n
        assert size % 4096 == 0
        if count:
            self.sent[name] = self.sent.get(name, 0) + size // 4096

    def tiles(self, sem, tiles):
        room = self.room.at[pl.ds(0, tiles)]
        return pltpu.make_async_remote_copy(
            src_ref=room,
            dst_ref=room,
            send_sem=self.send,
            recv_sem=sem,
            device_id=self.other,
            device_id_type=MESH,
        )

    def wait(self, name):
        assert name not in self.waited
        self.waited[name] = self.sent[name]
        self.tiles(self.sem(name), self.sent[name]).wait_recv()

    def drain(self):
        assert self.waited == self.sent
        total = sum(self.sent.values())
        assert (len(self.names), total) == (SEMS, TILES), (len(self.names), total)
        self.tiles(self.recv.at[0], total).wait_send()


def dot(a, b):
    return jnp.dot(a, b, preferred_element_type=f32)


def kernel(
    x_hbm, qg_hbm, fg_hbm, fp_hbm, lb_hbm, rq_hbm, rf_hbm, cq_hbm, cf_hbm,
    outer_ref, pre_ref, col_ref,
    x_ref, qg_ref, fg_ref, fp_ref, lb_ref, rq_ref, rf_ref, cq_ref, cf_ref,
    xt, xx, gx, rpack, rin, pmine, pout, pin, gp, rd, ru, sb, rf, gz, gc, o, orv, lp, lin, gram, gin, col, colin, sq, sqx, sqy,
    room, send, recv, loads,
):
    z, x, k, y = (lax.axis_index(n) for n in ("fs_0", "fs_1", "fs_2", "tp"))
    ko = 1 - k
    at = lambda v, n, m: lax.rem(v + n + m, m)
    ym, yp, y2 = at(y, -1, 4), at(y, 1, 4), at(y, 2, 4)
    zat = lambda n: at(z, n, 16)
    net = Net(send, recv, room, dict(fs_2=ko))
    steps = (2, 1, 3)
    plane = [
        (dx, dy, kk)
        for dx, dy in ((2, 2), (1, 2), (3, 2), (2, 1), (2, 3), (1, 1), (3, 3), (1, 3), (3, 1), (2, 0), (0, 2), (1, 0), (0, 1), (3, 0), (0, 3), (0, 0))
        for kk in (k, ko)
        if (dx, dy) != (0, 0) or kk is ko
    ]

    barrier = pltpu.get_barrier_semaphore()
    partners = [dict(fs_1=at(x, dx, 4), tp=at(y, dy, 4), fs_2=kk) for dx, dy, kk in plane]
    partners += [dict(fs_0=zat(n)) for n in (6, -6, 3, -3, 2, -2, 1, -1)]
    for who in partners:
        pl.semaphore_signal(barrier, inc=1, device_id=who, device_id_type=MESH)

    pairs = (
        (x_hbm, x_ref), (qg_hbm, qg_ref), (fg_hbm, fg_ref), (fp_hbm, fp_ref), (lb_hbm, lb_ref),
        (rq_hbm, rq_ref), (rf_hbm, rf_ref), (cq_hbm, cq_ref), (cf_hbm, cf_ref),
    )
    load = [pltpu.make_async_copy(u, v, loads.at[n]) for n, (u, v) in enumerate(pairs)]
    for c in load:
        c.start()
    load[0].wait()
    for n in range(4):
        turned = x_ref[:, n * 128 : (n + 1) * 128].T
        for q in range(4):
            xt[q, n * 32 : (n + 1) * 32] = turned[q * 32 : (q + 1) * 32]
    xx[y, x] = xt[x]
    for c in load[1:5]:
        c.wait()
    gx[x, 0] = qg_ref[...]
    gate = jax.nn.sigmoid(fp_ref[...].astype(f32))
    gx[x, 1] = (fg_ref[...].astype(f32) * (1.0 - lb_ref[...]) * gate * (1.0 - gate)).astype(bf16)
    for c in load[5:]:
        c.wait()
    for m, ref in enumerate((rq_ref, rf_ref)):
        for n in range(4):
            wide = ref[:, n * 512 : (n + 1) * 512].astype(f32)
            for q in range(4):
                strips = [wide[:, w * 128 + q * 32 : w * 128 + (q + 1) * 32] for w in range(4)]
                rpack[m, q, n] = jnp.concatenate(strips, axis=1).astype(bf16)
    rin[x, k] = rpack[k, x]
    pl.semaphore_wait(barrier, len(partners))

    for d in steps:
        net.copy(("x", d), xt.at[at(x, d, 4)], xx.at[y, x], fs_1=at(x, d, 4))

    def ysend(n):
        for d in steps:
            net.copy(("y", d), xx.at[y, n], xx.at[y, n], tp=at(y, d, 4))

    ysend(x)
    for d in steps:
        net.copy("g", gx.at[x], gx.at[x], fs_1=at(x, d, 4))
    net.copy("r", rpack.at[ko, x], rin.at[x, k], fs_2=ko)
    for d in (1, 3, 2):
        net.wait(("x", d))
        ysend(at(x, -d, 4))

    def product(j, a):
        lhs = jnp.concatenate([xx[a, n] for n in range(4)], axis=1)
        pout[a] = dot(lhs, gx[:, ko].reshape(512, 256))
        pmine[a] = dot(lhs, gx[:, k].reshape(512, 256)).reshape(4, 32, 256)
        net.copy(("p", j), pout.at[a], pin.at[a], fs_2=ko)

    def scatter(j, a):
        net.wait(("p", j))
        total = pmine[a] + pin[a].reshape(4, 32, 256)
        pmine[a] = total
        gp[a] = total.astype(bf16)
        for q in range(4):
            t = 4 * a + q
            d = at(t, -z, 16)
            up = (d == 4) | (d == 5) | (d == 7) | (d == 8)
            down = (d == 9) | (d == 11) | (d == 12)
            direct = (d == 1) | (d == 2) | (d == 3) | (d == 13) | (d == 14) | (d == 15)

            @pl.when(up | down)
            def _():
                slot = d - jnp.where(up, 4, 3)
                relay = lax.rem(t + jnp.where(up, 10, 6), 16)
                net.copy("u", gp.at[a, q], ru.at[slot], count=False, fs_0=relay)

            @pl.when(direct)
            def _():
                net.copy("s", gp.at[a, q], rd.at[lax.rem(d + 3, 16)], count=False, fs_0=t)

    net.wait("g")
    product(0, y)
    net.wait(("y", 1))
    product(1, ym)
    net.wait(("y", 3))
    product(2, yp)
    scatter(0, y)
    net.wait(("y", 2))
    product(3, y2)
    scatter(1, ym)
    scatter(2, yp)
    scatter(3, y2)
    for dx in steps:
        for m, kk in ((k, k), (ko, ko)):
            net.copy("r", rpack.at[m, at(x, dx, 4)], rin.at[x, k], fs_1=at(x, dx, 4), fs_2=kk)
    net.sent["s"], net.sent["u"] = 6 * 4, 7 * 4
    net.wait("u")
    part = lambda t: pmine[t // 4, lax.rem(t, 4)]
    for n, to, slots in ((0, zat(6), (0, 1, 3, 4)), (1, zat(-6), (6, 8, 9))):
        total = part(to)
        for i in slots:
            total = total + ru[i].astype(f32)
        sb[n] = total.astype(bf16)
        net.copy("f", sb.at[n], rf.at[n], fs_0=to)
    net.wait("s")
    total = part(z)
    for i in (0, 1, 2, 4, 5, 6):
        total = total + rd[i].astype(f32)
    net.wait("f")
    total = total + rf[0].astype(f32) + rf[1].astype(f32)
    mine = total.astype(bf16)
    gc[z] = mine
    gz[x] = mine

    chunks = ((0, 1, -1, 2), (-2, 3, -3, 6), (-6, -7, -5, 5), (7, -8, -4, 4))

    def zsend(name, e, n):
        net.copy(("z", name), gc.at[zat(e)], gc.at[zat(e)], fs_0=zat(n))

    for n in (6, -6):
        zsend(-n, 0, n)
    for n in (3, -3, 2, -2, 1, -1):
        zsend("direct", 0, n)
    for d in steps:
        net.copy("gz", gz.at[x], gz.at[x], fs_1=at(x, d, 4))
    net.wait("r")
    net.wait(("z", 6))
    for n in (2, 1, -1):
        zsend("relay", 6, n)
    net.wait(("z", -6))
    for n in (2, -2, 1, -1):
        zsend("relay", -6, n)
    net.wait(("z", "direct"))
    net.wait("gz")
    rows = gz[...].reshape(128, 256)

    def outer(i):
        cols = jnp.concatenate([gc[zat(e)] for e in chunks[i]], axis=0)
        block = lax.dot_general(rows, cols, (((1,), (1,)), ((), ())), preferred_element_type=f32).astype(bf16)
        for q in range(8):
            o[q // 2, q % 2, i] = block[q * 16 : (q + 1) * 16]

    def osend(h):
        orv[k, x, y, h] = o[x, k, h]
        for dx, dy, kk in plane:
            to_x, to_y = at(x, dx, 4), at(y, dy, 4)
            net.copy("o", o.at[to_x, kk, h], orv.at[k, x, y, h], fs_1=to_x, tp=to_y, fs_2=kk)

    outer(0)
    outer(1)
    osend(pl.ds(0, 2))
    net.wait(("z", "relay"))
    whole = gc[...].reshape(512, 256)
    wide = whole.astype(f32)
    square = jnp.sum((wide * wide).reshape(64, 8, 256), axis=0)
    sq[...] = jnp.broadcast_to(jnp.sum(square, axis=(0, 1), keepdims=True), (8, 128))
    sqx[x] = sq[...]
    for h in range(2):
        lanes = slice(h * 128, (h + 1) * 128)
        turned = whole[:, lanes]
        gram[h] = lax.dot_general(turned, turned, (((0,), (0,)), ((), ())), preferred_element_type=f32).astype(bf16)
    for d in steps:
        net.copy("q", sq, sqx.at[x], fs_1=at(x, d, 4))
        net.copy("gram", gram, gin.at[x], fs_1=at(x, d, 4))
    outer(2)
    outer(3)
    osend(pl.ds(2, 2))
    roots = rin[...].reshape(8, 4, 16, 128)
    roots = jnp.concatenate(
        [jnp.concatenate([roots[q, n] for n in range(4)], axis=1) for q in range(8)], axis=0
    )
    left = dot(roots, whole)
    lp[...] = left.reshape(4, 2, 16, 256)
    lin[k, x] = lp[x, k]
    for dx in (2, 1, 3, 0):
        for kk in (k, ko):
            if dx or kk is ko:
                to_x = at(x, dx, 4)
                net.copy("l", lp.at[to_x, kk], lin.at[k, x], fs_1=to_x, fs_2=kk)
    net.wait("q")
    total = sqx[0] + sqx[1] + sqx[2] + sqx[3]
    sq2 = sqy.at[k, y]
    sq2[...] = total
    for d in steps:
        for kk in (k, ko):
            net.copy("sqy", sqy.at[k, y], sqy.at[k, y], tp=at(y, d, 4), fs_2=kk)
    net.copy("sqy", sqy.at[k, y], sqy.at[k, y], fs_2=ko)
    net.wait("gram")
    gin[x] = gram[...]
    col[...] = gin[0].astype(f32) + gin[1].astype(f32) + gin[2].astype(f32) + gin[3].astype(f32)
    net.copy("col", col, colin.at[k], fs_2=ko)
    colin[k] = col[...]
    net.wait("l")
    pre = {}
    for m, ref in enumerate((cq_ref, cf_ref)):
        value = lin[m, 0] + lin[m, 1] + lin[m, 2] + lin[m, 3]
        high = value.astype(bf16)
        low = (value - high.astype(f32)).astype(bf16)
        for h in range(2):
            lanes = slice(h * 128, (h + 1) * 128)
            pre[m, h] = dot(high[:, lanes], ref[h]) + dot(low[:, lanes], ref[h])
    net.wait("o")
    net.wait("col")
    net.wait("sqy")
    lane = lax.broadcasted_iota(jnp.int32, (16, 128), 1) // 32
    for m in range(2):
        square = sqy[m, 0] + sqy[m, 1] + sqy[m, 2] + sqy[m, 3]
        scale = jnp.sqrt(D * HW / (square + 1.0))[:1]
        twice = scale * scale
        by_row = (1.0 - stat_decay) / HW * twice
        by_col = (1.0 - stat_decay) / D * twice
        for i in range(4):
            sums = []
            for n in range(4):
                total = orv[m, n, 0, i].astype(f32)
                for q in range(1, 4):
                    total = total + orv[m, n, q, i].astype(f32)
                sums.append(by_row * total)
            for e in range(4):
                block = sums[0] if e == 0 else pltpu.roll(sums[0], (128 - 32 * e) % 128, 1)
                for n in range(1, 4):
                    turn = (32 * (n - e)) % 128
                    block = jnp.where(lane == n, pltpu.roll(sums[n], turn, 1) if turn else sums[n], block)
                lanes = pl.ds(pl.multiple_of(zat(chunks[i][e]) * 128, 128), 128)
                outer_ref[m, :, lanes] = block
        for h in range(2):
            lanes = slice(h * 128, (h + 1) * 128)
            pre_ref[m, :, lanes] = scale * pre[m, h]
            col_ref[m, h] = by_col * colin[m, h]
    net.drain()


def exchange(inputs, qg, fg, fp, lb, rq, rf, cq, cf):
    vm = pl.BlockSpec(memory_space=pltpu.VMEM)
    hbm = pl.BlockSpec(memory_space=pltpu.HBM)
    s = lambda shape, kind=bf16: pltpu.VMEM(shape, kind)
    given = (inputs, qg, fg, fp, lb.reshape(1, -1), rq, rf, cq, cf)
    return pl.pallas_call(
        kernel,
        out_shape=(
            pltpu.VMEM((2, 16, D), f32),
            pltpu.VMEM((2, 16, 256), f32),
            pltpu.VMEM((2, 2, HEAD, HEAD), f32),
        ),
        in_specs=[hbm] * 9,
        out_specs=(vm,) * 3,
        scratch_shapes=[s(v.shape, v.dtype) for v in given]
        + [
            s((4, 128, 128)),
            s((4, 4, 128, 128)),
            s((4, 2, 128, 256)),
            s((2, 4, 4, 16, 128)),
            s((4, 2, 4, 16, 128)),
            s((4, 4, 32, 256), f32),
            s((4, 128, 256), f32),
            s((4, 128, 256), f32),
            s((4, 4, 32, 256)),
            s((7, 32, 256)),
            s((10, 32, 256)),
            s((2, 32, 256)),
            s((2, 32, 256)),
            s((4, 32, 256)),
            s((16, 32, 256)),
            s((4, 2, 4, 16, 128)),
            s((2, 4, 4, 4, 16, 128)),
            s((4, 2, 16, 256), f32),
            s((2, 4, 16, 256), f32),
            s((2, HEAD, HEAD)),
            s((4, 2, HEAD, HEAD)),
            s((2, HEAD, HEAD), f32),
            s((2, 2, HEAD, HEAD), f32),
            s((8, 128), f32),
            s((4, 8, 128), f32),
            s((2, 4, 8, 128), f32),
            s((TILES, 16, 128)),
            pltpu.SemaphoreType.DMA,
            pltpu.SemaphoreType.DMA((SEMS,)),
            pltpu.SemaphoreType.DMA((len(given),)),
        ],
        compiler_params=pltpu.CompilerParams(collective_id=0, has_side_effects=True),
        name="exchange",
    )(*given)


def finish(weight, moment, rows, cols, outer, precond, col):
    rows_next = stat_decay * rows + outer
    cols_next = stat_decay * cols + col
    moment_next = moment_decay * moment + (1.0 - moment_decay) * precond
    step = moment_decay * moment_next + (1.0 - moment_decay) * precond
    master = weight - learn_rate * step
    return (master, master.astype(bf16), step, moment_next, rows_next, cols_next)


def on_device(inputs, qg, fg, fp, lb, qw, fw, qm, fm, qr, fr, qc, fc, qrr, frr, qcr, fcr):
    outer, pre, col = exchange(inputs, qg, fg, fp, lb, qrr, frr, qcr, fcr)
    q = finish(qw, qm, qr, qc, outer[0], pre[0], col[0])
    f = finish(fw, fm, fr, fc, outer[1], pre[1], col[1])
    return tuple(v for pair in zip(q, f) for v in pair)


def solution(mesh):
    split = Mesh(mesh.devices.reshape(16, 4, 2, mesh.shape["tp"]), ("fs_0", "fs_1", "fs_2", "tp"))
    both, rows, cols = P(FS, "tp"), P(FS, None), P("tp", None, None)
    return jax.shard_map(
        on_device,
        mesh=split,
        in_specs=(both,) * 4 + (P("tp"),) + (both,) * 4 + (rows,) * 2 + (cols,) * 2 + (rows,) * 2 + (cols,) * 2,
        out_specs=(both,) * 8 + (rows,) * 2 + (cols,) * 2,
        check_vma=False,
    )
```

time: 71.3 us -> 66.2 us (0.928)
  Pallas kernels: 67.7 us -> 62.6 us
    pallas_call x1, Pallas kernels: 67.7 us -> 62.6 us  [exchange(): pl.pallas_call(kernel, out_shape=(pltpu.VMEM((2, 16, D), f32), pltpu.VMEM...]
where the time goes in v3:
time: 66.2 us; the launch traced here: 66 us
  Pallas kernels  62.6 us (95%)
  other arithmetic  2.12 us (3%)
  between operations  0.74 us (1%)
    pallas_call x1, Pallas kernels, exchange(): pl.pallas_call(kernel, out_shape=(pltpu.VMEM((2, 16, D), f32), pltpu.VMEM...  62.6 us

profile of v3, /device:TPU:1, one launch (start us, length us, event | category | flops | bytes accessed | tf_op | source)
XLA Modules:
  0.0 66.0 jit_solution(18298018522168264385)
XLA Ops:
  0.6 0.0 copy-start.4
  0.7 0.0 copy-start.5
  0.7 0.0 copy-start.6
  0.7 0.0 copy-start.7
  0.7 0.0 copy-start.1
  0.7 62.6 %exchange.1 = (f32[2,16,2048]{2,1,0:T(8,128)S(1)}, f32[2,16,256]{2,1,0:T(8,128)S(1)}, f32[2,2,128,128]{3,2,1,0:T(8,128)S(1)}) custom-call(bf16[128,512]{1,0:T(8,128)(2,1)} %x_hbm.1, bf16[128,256]{1,0:T(8,128)(2,1)} %qg_hbm.1, bf16[128,256]{1,0:T(8,128)(2,1)} %fg_hbm.1, bf16[128,256]{1,0:T(8,128)(2,1)} %fp_hbm.1, f32[1,256]{1,0:T(1,128)} %bitcast.19, ...), custom_call_target="tpu_custom_call" | custom-call | tf_op jit(solution)/shard_map/exchange/pallas_call | solution.py:332
  63.3 0.0 copy-start
  63.3 0.0 copy-done.4
  63.3 0.0 copy-done.5
  63.3 0.0 copy-done.6
  63.3 0.0 copy-done.7
  63.4 0.7 fusion
  64.0 0.0 copy-done.1
  64.0 0.2 copy-done
  64.2 0.0 copy-start.2
  64.2 0.0 copy-start.3
  64.2 0.7 %bitcast_add_fusion.2 = (f32[16,2048]{1,0:T(8,128)}, f32[16,2048]{1,0:T(8,128)}) fusion(f32[2,16,2048]{2,1,0:T(8,128)S(1)} %get-tuple-element.16, f32[16,2048]{1,0:T(8,128)S(1)} %copy-done, f32[16,2048]{1,0:T(8,128)S(1)} %copy-done.1), kind=kLoop, calls=%fused_computation.2 | loop fusion | flops 131072 | bytes 786432 | tf_op jit(solution)/shard_map/add | solution.py:380
  65.0 0.2 copy-done.2
  65.1 0.1 copy-done.3
  65.3 0.7 %bitcast_add_fusion = (f32[2,128,128]{2,1,0:T(8,128)}, f32[2,128,128]{2,1,0:T(8,128)}) fusion(f32[2,2,128,128]{3,2,1,0:T(8,128)S(1)} %get-tuple-element.17, f32[2,128,128]{2,1,0:T(8,128)S(1)} %copy-done.2, f32[2,128,128]{2,1,0:T(8,128)S(1)} %copy-done.3), kind=kLoop, calls=%fused_computation | loop fusion | flops 131072 | bytes 786432 | tf_op jit(solution)/shard_map/add | solution.py:381
Async XLA Ops:
  0.6 62.7 %copy-start.4 = (f32[16,256]{1,0:T(8,128)S(1)}, f32[16,256]{1,0:T(8,128)}, u32[]{:S(2)}) copy-start(f32[16,256]{1,0:T(8,128)} %param.23) | copy-start | bytes 49156
  0.7 62.7 %copy-start.5 = (f32[16,256]{1,0:T(8,128)S(1)}, f32[16,256]{1,0:T(8,128)}, u32[]{:S(2)}) copy-start(f32[16,256]{1,0:T(8,128)} %param.25) | copy-start | bytes 49156
  0.7 62.7 %copy-start.6 = (f32[16,256]{1,0:T(8,128)S(1)}, f32[16,256]{1,0:T(8,128)}, u32[]{:S(2)}) copy-start(f32[16,256]{1,0:T(8,128)} %param.22) | copy-start | bytes 49156
  0.7 62.7 %copy-start.7 = (f32[16,256]{1,0:T(8,128)S(1)}, f32[16,256]{1,0:T(8,128)}, u32[]{:S(2)}) copy-start(f32[16,256]{1,0:T(8,128)} %param.24) | copy-start | bytes 49156
  0.7 63.3 %copy-start.1 = (f32[16,2048]{1,0:T(8,128)S(1)}, f32[16,2048]{1,0:T(8,128)}, u32[]{:S(2)}) copy-start(f32[16,2048]{1,0:T(8,128)} %param.26) | copy-start | bytes 393220
  63.3 0.9 %copy-start = (f32[16,2048]{1,0:T(8,128)S(1)}, f32[16,2048]{1,0:T(8,128)}, u32[]{:S(2)}) copy-start(f32[16,2048]{1,0:T(8,128)} %param.27) | copy-start | bytes 393220
  64.2 0.9 %copy-start.2 = (f32[2,128,128]{2,1,0:T(8,128)S(1)}, f32[2,128,128]{2,1,0:T(8,128)}, u32[]{:S(2)}) copy-start(f32[2,128,128]{2,1,0:T(8,128)} %param.29) | copy-start | bytes 393220
  64.2 1.1 %copy-start.3 = (f32[2,128,128]{2,1,0:T(8,128)S(1)}, f32[2,128,128]{2,1,0:T(8,128)}, u32[]{:S(2)}) copy-start(f32[2,128,128]{2,1,0:T(8,128)} %param.28) | copy-start | bytes 393220

commit v4 on v3

--- a/solution.py
+++ b/solution.py
@@ -11,8 +11,8 @@
 HEAD = 128
 FS = ("fs_0", "fs_1", "fs_2")
 MESH = pl.DeviceIdType.MESH
-SEMS = 26
-TILES = 746
+SEMS = 22
+TILES = 698
 
 stat_decay = 0.9
 moment_decay = 0.9
@@ -74,14 +74,18 @@
 
 
 def kernel(
-    x_hbm, qg_hbm, fg_hbm, fp_hbm, lb_hbm, rq_hbm, rf_hbm, cq_hbm, cf_hbm,
-    outer_ref, pre_ref, col_ref,
-    x_ref, qg_ref, fg_ref, fp_ref, lb_ref, rq_ref, rf_ref, cq_ref, cf_ref,
-    xt, xx, gx, rpack, rin, pmine, pout, pin, gp, rd, ru, sb, rf, gz, gc, o, orv, lp, lin, gram, gin, col, colin, sq, sqx, sqy,
+    *refs,
+):
+    given, refs = refs[:17], refs[17:]
+    made, refs = refs[:12], refs[12:]
+    held, refs = refs[:17], refs[17:]
+    x_ref, qg_ref, fg_ref, fp_ref, lb_ref, rq_ref, rf_ref, cq_ref, cf_ref = held[:9]
+    (
+    xt, xx, gx, rpack, rin, pmine, pout, pin, gp, rd, ru, sb, rf, gz, gc, o, orv, lp, lin, gram, gin, quarter, colin, sq, sqx, sqsem,
     room, send, recv, loads,
-):
+    ) = refs
     z, x, k, y = (lax.axis_index(n) for n in ("fs_0", "fs_1", "fs_2", "tp"))
-    ko = 1 - k
+    ko, b = 1 - k, lax.rem(z, 2)
     at = lambda v, n, m: lax.rem(v + n + m, m)
     ym, yp, y2 = at(y, -1, 4), at(y, 1, 4), at(y, 2, 4)
     zat = lambda n: at(z, n, 16)
@@ -96,15 +100,12 @@
 
     barrier = pltpu.get_barrier_semaphore()
     partners = [dict(fs_1=at(x, dx, 4), tp=at(y, dy, 4), fs_2=kk) for dx, dy, kk in plane]
-    partners += [dict(fs_0=zat(n)) for n in (6, -6, 3, -3, 2, -2, 1, -1)]
+    partners += [dict(fs_0=zat(n)) for n in (6, -6, 4, -4, 3, -3, 2, -2, 1, -1)]
+    partners += [dict(fs_0=zat(n), fs_2=ko) for n in (1, -1)]
     for who in partners:
         pl.semaphore_signal(barrier, inc=1, device_id=who, device_id_type=MESH)
 
-    pairs = (
-        (x_hbm, x_ref), (qg_hbm, qg_ref), (fg_hbm, fg_ref), (fp_hbm, fp_ref), (lb_hbm, lb_ref),
-        (rq_hbm, rq_ref), (rf_hbm, rf_ref), (cq_hbm, cq_ref), (cf_hbm, cf_ref),
-    )
-    load = [pltpu.make_async_copy(u, v, loads.at[n]) for n, (u, v) in enumerate(pairs)]
+    load = [pltpu.make_async_copy(u, v, loads.at[n]) for n, (u, v) in enumerate(zip(given, held))]
     for c in load:
         c.start()
     load[0].wait()
@@ -118,7 +119,19 @@
     gx[x, 0] = qg_ref[...]
     gate = jax.nn.sigmoid(fp_ref[...].astype(f32))
     gx[x, 1] = (fg_ref[...].astype(f32) * (1.0 - lb_ref[...]) * gate * (1.0 - gate)).astype(bf16)
-    for c in load[5:]:
+    pl.semaphore_wait(barrier, len(partners))
+
+    for d in steps:
+        net.copy(("x", d), xt.at[at(x, d, 4)], xx.at[y, x], fs_1=at(x, d, 4))
+
+    def ysend(n):
+        for d in steps:
+            net.copy(("y", d), xx.at[y, n], xx.at[y, n], tp=at(y, d, 4))
+
+    ysend(x)
+    for d in steps:
+        net.copy("g", gx.at[x], gx.at[x], fs_1=at(x, d, 4))
+    for c in load[5:9]:
         c.wait()
     for m, ref in enumerate((rq_ref, rf_ref)):
         for n in range(4):
@@ -127,18 +140,6 @@
                 strips = [wide[:, w * 128 + q * 32 : w * 128 + (q + 1) * 32] for w in range(4)]
                 rpack[m, q, n] = jnp.concatenate(strips, axis=1).astype(bf16)
     rin[x, k] = rpack[k, x]
-    pl.semaphore_wait(barrier, len(partners))
-
-    for d in steps:
-        net.copy(("x", d), xt.at[at(x, d, 4)], xx.at[y, x], fs_1=at(x, d, 4))
-
-    def ysend(n):
-        for d in steps:
-            net.copy(("y", d), xx.at[y, n], xx.at[y, n], tp=at(y, d, 4))
-
-    ysend(x)
-    for d in steps:
-        net.copy("g", gx.at[x], gx.at[x], fs_1=at(x, d, 4))
     net.copy("r", rpack.at[ko, x], rin.at[x, k], fs_2=ko)
     for d in (1, 3, 2):
         net.wait(("x", d))
@@ -190,41 +191,42 @@
     net.sent["s"], net.sent["u"] = 6 * 4, 7 * 4
     net.wait("u")
     part = lambda t: pmine[t // 4, lax.rem(t, 4)]
-    for n, to, slots in ((0, zat(6), (0, 1, 3, 4)), (1, zat(-6), (6, 8, 9))):
-        total = part(to)
+    for n, e, slots in ((0, 6, (0, 1, 3, 4)), (1, -6, (6, 8, 9))):
+        total = part(zat(e))
         for i in slots:
             total = total + ru[i].astype(f32)
         sb[n] = total.astype(bf16)
-        net.copy("f", sb.at[n], rf.at[n], fs_0=to)
+        net.copy("f", sb.at[n], rf.at[2 + 2 * n], fs_0=zat(e))
+        net.copy("f", sb.at[n], rf.at[3 + 2 * n], fs_0=zat(2 * e))
     net.wait("s")
     total = part(z)
     for i in (0, 1, 2, 4, 5, 6):
         total = total + rd[i].astype(f32)
+    sb[2] = total.astype(bf16)
+    net.copy("f", sb.at[2], rf.at[0], fs_0=zat(6))
+    net.copy("f", sb.at[2], rf.at[1], fs_0=zat(-6))
     net.wait("f")
-    total = total + rf[0].astype(f32) + rf[1].astype(f32)
-    mine = total.astype(bf16)
+
+    def joined(mid, above, below):
+        return (mid.astype(f32) + above.astype(f32) + below.astype(f32)).astype(bf16)
+
+    mine = joined(sb[2], rf[4], rf[2])
     gc[z] = mine
     gz[x] = mine
-
-    chunks = ((0, 1, -1, 2), (-2, 3, -3, 6), (-6, -7, -5, 5), (7, -8, -4, 4))
-
-    def zsend(name, e, n):
-        net.copy(("z", name), gc.at[zat(e)], gc.at[zat(e)], fs_0=zat(n))
-
-    for n in (6, -6):
-        zsend(-n, 0, n)
-    for n in (3, -3, 2, -2, 1, -1):
-        zsend("direct", 0, n)
+    gc[zat(6)] = joined(rf[1], rf[5], sb[0])
+    gc[zat(-6)] = joined(rf[0], sb[1], rf[3])
+
+    chunks = ((0, 6, -6, 1), (7, -5, -1, 5), (-7, 2, -8, -4), (-2, 4, 3, -3))
     for d in steps:
         net.copy("gz", gz.at[x], gz.at[x], fs_1=at(x, d, 4))
+    for name, n, held_here in (
+        ("first", 1, (0, 6, -6)), ("first", -1, (0, 6, -6)), ("last", 3, (0,)), ("last", -3, (0,)),
+        ("last", 2, (0, 6, -6)), ("last", -2, (0, -6)),
+    ):
+        for e in held_here:
+            net.copy(("z", name), gc.at[zat(e)], gc.at[zat(e)], fs_0=zat(n))
     net.wait("r")
-    net.wait(("z", 6))
-    for n in (2, 1, -1):
-        zsend("relay", 6, n)
-    net.wait(("z", -6))
-    for n in (2, -2, 1, -1):
-        zsend("relay", -6, n)
-    net.wait(("z", "direct"))
+    net.wait(("z", "first"))
     net.wait("gz")
     rows = gz[...].reshape(128, 256)
 
@@ -243,63 +245,90 @@
     outer(0)
     outer(1)
     osend(pl.ds(0, 2))
-    net.wait(("z", "relay"))
+    net.wait(("z", "last"))
     whole = gc[...].reshape(512, 256)
-    wide = whole.astype(f32)
-    square = jnp.sum((wide * wide).reshape(64, 8, 256), axis=0)
-    sq[...] = jnp.broadcast_to(jnp.sum(square, axis=(0, 1), keepdims=True), (8, 128))
-    sqx[x] = sq[...]
     for h in range(2):
         lanes = slice(h * 128, (h + 1) * 128)
         turned = whole[:, lanes]
-        gram[h] = lax.dot_general(turned, turned, (((0,), (0,)), ((), ())), preferred_element_type=f32).astype(bf16)
+        both = lax.dot_general(turned, turned, (((0,), (0,)), ((), ())), preferred_element_type=f32).astype(bf16)
+        gram[h, 0] = both[:64]
+        gram[h, 1] = both[64:]
     for d in steps:
-        net.copy("q", sq, sqx.at[x], fs_1=at(x, d, 4))
-        net.copy("gram", gram, gin.at[x], fs_1=at(x, d, 4))
+        net.copy("gram", gram.at[b], gin.at[x], fs_1=at(x, d, 4))
+    wide = whole.astype(f32)
+    square = jnp.sum((wide * wide).reshape(64, 8, 256), axis=0)
+    square = jnp.sum(square, axis=(0, 1), keepdims=True)
+    sq[0] = jnp.broadcast_to(square, (1, 128))
     outer(2)
     outer(3)
+    for n, (dx, dy, kk) in enumerate(plane):
+        pltpu.make_async_remote_copy(
+            src_ref=sq.at[0],
+            dst_ref=sqx.at[n],
+            send_sem=sqsem.at[0],
+            recv_sem=sqsem.at[1],
+            device_id=dict(fs_1=at(x, dx, 4), tp=at(y, dy, 4), fs_2=kk),
+            device_id_type=MESH,
+        ).start()
     osend(pl.ds(2, 2))
     roots = rin[...].reshape(8, 4, 16, 128)
     roots = jnp.concatenate(
         [jnp.concatenate([roots[q, n] for n in range(4)], axis=1) for q in range(8)], axis=0
     )
     left = dot(roots, whole)
-    lp[...] = left.reshape(4, 2, 16, 256)
+    lp[...] = left.reshape(4, 2, 16, 256).astype(bf16)
     lin[k, x] = lp[x, k]
     for dx in (2, 1, 3, 0):
         for kk in (k, ko):
             if dx or kk is ko:
                 to_x = at(x, dx, 4)
                 net.copy("l", lp.at[to_x, kk], lin.at[k, x], fs_1=to_x, fs_2=kk)
-    net.wait("q")
-    total = sqx[0] + sqx[1] + sqx[2] + sqx[3]
-    sq2 = sqy.at[k, y]
-    sq2[...] = total
-    for d in steps:
+    net.wait("gram")
+    gin[x] = gram[b]
+    total = gin[0].astype(f32) + gin[1].astype(f32) + gin[2].astype(f32) + gin[3].astype(f32)
+    quarter[...] = total.astype(bf16)
+    for n, e in ((0, 1), (1, -1)):
         for kk in (k, ko):
-            net.copy("sqy", sqy.at[k, y], sqy.at[k, y], tp=at(y, d, 4), fs_2=kk)
-    net.copy("sqy", sqy.at[k, y], sqy.at[k, y], fs_2=ko)
-    net.wait("gram")
-    gin[x] = gram[...]
-    col[...] = gin[0].astype(f32) + gin[1].astype(f32) + gin[2].astype(f32) + gin[3].astype(f32)
-    net.copy("col", col, colin.at[k], fs_2=ko)
-    colin[k] = col[...]
+            net.copy("col", quarter.at[n], colin.at[k, b, n], fs_0=zat(e), fs_2=kk)
+    net.copy("col", quarter, colin.at[k, b], fs_2=ko)
+    colin[k, b] = quarter[...]
     net.wait("l")
     pre = {}
     for m, ref in enumerate((cq_ref, cf_ref)):
-        value = lin[m, 0] + lin[m, 1] + lin[m, 2] + lin[m, 3]
+        value = lin[m, 0].astype(f32)
+        for n in range(1, 4):
+            value = value + lin[m, n].astype(f32)
         high = value.astype(bf16)
         low = (value - high.astype(f32)).astype(bf16)
         for h in range(2):
             lanes = slice(h * 128, (h + 1) * 128)
             pre[m, h] = dot(high[:, lanes], ref[h]) + dot(low[:, lanes], ref[h])
+    for c in load[9:]:
+        c.wait()
     net.wait("o")
     net.wait("col")
-    net.wait("sqy")
+    squares = pltpu.make_async_remote_copy(
+        src_ref=sqx,
+        dst_ref=sqx,
+        send_sem=sqsem.at[0],
+        recv_sem=sqsem.at[1],
+        device_id=dict(fs_2=ko),
+        device_id_type=MESH,
+    )
+    squares.wait_recv()
+    squares.wait_send()
+    same, cross = sq[0], jnp.zeros((1, 128), f32)
+    for n, (dx, dy, kk) in enumerate(plane):
+        if kk is k:
+            same = same + sqx[n]
+        else:
+            cross = cross + sqx[n]
     lane = lax.broadcasted_iota(jnp.int32, (16, 128), 1) // 32
     for m in range(2):
-        square = sqy[m, 0] + sqy[m, 1] + sqy[m, 2] + sqy[m, 3]
-        scale = jnp.sqrt(D * HW / (square + 1.0))[:1]
+        master_ref, copy_ref, step_ref, moment_ref, rows_ref, cols_ref = made[m::2]
+        weight_old, moment_old, rows_old, cols_old = held[9 + m :: 2]
+        square = jnp.where(k == m, same, cross)
+        scale = jnp.sqrt(D * HW / (square + 1.0))
         twice = scale * scale
         by_row = (1.0 - stat_decay) / HW * twice
         by_col = (1.0 - stat_decay) / D * twice
@@ -316,28 +345,44 @@
                     turn = (32 * (n - e)) % 128
                     block = jnp.where(lane == n, pltpu.roll(sums[n], turn, 1) if turn else sums[n], block)
                 lanes = pl.ds(pl.multiple_of(zat(chunks[i][e]) * 128, 128), 128)
-                outer_ref[m, :, lanes] = block
+                rows_ref[:, lanes] = stat_decay * rows_old[:, lanes] + block
         for h in range(2):
             lanes = slice(h * 128, (h + 1) * 128)
-            pre_ref[m, :, lanes] = scale * pre[m, h]
-            col_ref[m, h] = by_col * colin[m, h]
+            precond = scale * pre[m, h]
+            moment = moment_decay * moment_old[:, lanes] + (1.0 - moment_decay) * precond
+            step = moment_decay * moment + (1.0 - moment_decay) * precond
+            master = weight_old[:, lanes] - learn_rate * step
+            moment_ref[:, lanes] = moment
+            step_ref[:, lanes] = step
+            master_ref[:, lanes] = master
+            copy_ref[:, lanes] = master.astype(bf16)
+            for n in range(2):
+                part = slice(64 * n, 64 * n + 64)
+                cols_ref[h, part] = stat_decay * cols_old[h, part] + by_col * colin[m, h, n].astype(f32)
     net.drain()
 
 
-def exchange(inputs, qg, fg, fp, lb, rq, rf, cq, cf):
+def store(*refs):
+    sems = refs[24]
+    moves = [pltpu.make_async_copy(u, v, sems.at[n]) for n, (u, v) in enumerate(zip(refs[:12], refs[12:24]))]
+    for c in moves:
+        c.start()
+    for c in moves:
+        c.wait()
+
+
+def on_device(inputs, qg, fg, fp, lb, qw, fw, qm, fm, qr, fr, qc, fc, qrr, frr, qcr, fcr):
+    hbm = pl.BlockSpec(memory_space=pltpu.HBM)
     vm = pl.BlockSpec(memory_space=pltpu.VMEM)
-    hbm = pl.BlockSpec(memory_space=pltpu.HBM)
     s = lambda shape, kind=bf16: pltpu.VMEM(shape, kind)
-    given = (inputs, qg, fg, fp, lb.reshape(1, -1), rq, rf, cq, cf)
-    return pl.pallas_call(
+    given = (inputs, qg, fg, fp, lb.reshape(1, -1), qrr, frr, qcr, fcr, qw, fw, qm, fm, qr, fr, qc, fc)
+    like = (qw, fw, qg, fg, qw, fw, qw, fw, qr, fr, qc, fc)
+    shapes = [(v.shape if v.ndim != 2 or v.shape[1] == D else (16, 256), v.dtype) for v in like]
+    made = pl.pallas_call(
         kernel,
-        out_shape=(
-            pltpu.VMEM((2, 16, D), f32),
-            pltpu.VMEM((2, 16, 256), f32),
-            pltpu.VMEM((2, 2, HEAD, HEAD), f32),
-        ),
-        in_specs=[hbm] * 9,
-        out_specs=(vm,) * 3,
+        out_shape=tuple(pltpu.VMEM(*v) for v in shapes),
+        in_specs=[hbm] * 17,
+        out_specs=(vm,) * 12,
         scratch_shapes=[s(v.shape, v.dtype) for v in given]
         + [
             s((4, 128, 128)),
@@ -351,21 +396,21 @@
             s((4, 4, 32, 256)),
             s((7, 32, 256)),
             s((10, 32, 256)),
-            s((2, 32, 256)),
-            s((2, 32, 256)),
+            s((3, 32, 256)),
+            s((6, 32, 256)),
             s((4, 32, 256)),
             s((16, 32, 256)),
             s((4, 2, 4, 16, 128)),
             s((2, 4, 4, 4, 16, 128)),
-            s((4, 2, 16, 256), f32),
-            s((2, 4, 16, 256), f32),
-            s((2, HEAD, HEAD)),
-            s((4, 2, HEAD, HEAD)),
-            s((2, HEAD, HEAD), f32),
-            s((2, 2, HEAD, HEAD), f32),
-            s((8, 128), f32),
-            s((4, 8, 128), f32),
-            s((2, 4, 8, 128), f32),
+            s((4, 2, 16, 256)),
+            s((2, 4, 16, 256)),
+            s((2, 2, 64, HEAD)),
+            s((4, 2, 64, HEAD)),
+            s((2, 64, HEAD)),
+            s((2, 2, 2, 64, HEAD)),
+            s((1, 1, 128), f32),
+            s((31, 1, 128), f32),
+            pltpu.SemaphoreType.DMA((2,)),
             s((TILES, 16, 128)),
             pltpu.SemaphoreType.DMA,
             pltpu.SemaphoreType.DMA((SEMS,)),
@@ -374,22 +419,14 @@
         compiler_params=pltpu.CompilerParams(collective_id=0, has_side_effects=True),
         name="exchange",
     )(*given)
-
-
-def finish(weight, moment, rows, cols, outer, precond, col):
-    rows_next = stat_decay * rows + outer
-    cols_next = stat_decay * cols + col
-    moment_next = moment_decay * moment + (1.0 - moment_decay) * precond
-    step = moment_decay * moment_next + (1.0 - moment_decay) * precond
-    master = weight - learn_rate * step
-    return (master, master.astype(bf16), step, moment_next, rows_next, cols_next)
-
-
-def on_device(inputs, qg, fg, fp, lb, qw, fw, qm, fm, qr, fr, qc, fc, qrr, frr, qcr, fcr):
-    outer, pre, col = exchange(inputs, qg, fg, fp, lb, qrr, frr, qcr, fcr)
-    q = finish(qw, qm, qr, qc, outer[0], pre[0], col[0])
-    f = finish(fw, fm, fr, fc, outer[1], pre[1], col[1])
-    return tuple(v for pair in zip(q, f) for v in pair)
+    return pl.pallas_call(
+        store,
+        out_shape=tuple(jax.ShapeDtypeStruct(*v) for v in shapes),
+        in_specs=[vm] * 12,
+        out_specs=(hbm,) * 12,
+        scratch_shapes=[pltpu.SemaphoreType.DMA((12,))],
+        name="store",
+    )(*(pltpu.with_memory_space_constraint(v, pltpu.VMEM) for v in made))
 
 
 def solution(mesh):

time: 66.2 us -> 62.3 us (0.941)
  other arithmetic: 2.12 us -> 0 us
  Pallas kernels: 62.6 us -> 61.5 us
    add x2 -> x0, other arithmetic: 1.47 us -> none  [the longest x1 0.73 us: finish(): cols_next = stat_decay * cols + col]
    pallas_call x1 -> x2, Pallas kernels: 62.6 us -> 61.5 us  [the longest x1 60.5 us: on_device(): pl.pallas_call(kernel, out_shape=tuple((pltpu.VMEM(*v) for v in shapes)),...]
where the time goes in v4:
time: 62.3 us; the launch traced here: 62.1 us
  Pallas kernels  61.5 us (99%)
  between operations  0.66 us (1%)
    pallas_call x1, Pallas kernels, on_device(): pl.pallas_call(kernel, out_shape=tuple((pltpu.VMEM(*v) for v in shapes)),...  60.5 us

profile of v4, /device:TPU:1, one launch (start us, length us, event | category | flops | bytes accessed | tf_op | source)
XLA Modules:
  0.0 62.1 jit_solution(7622099920632486791)
XLA Ops:
  0.7 60.5 %exchange.1 = (f32[16,256]{1,0:T(8,128)S(1)}, f32[16,256]{1,0:T(8,128)S(1)}, bf16[16,256]{1,0:T(8,128)(2,1)S(1)}, bf16[16,256]{1,0:T(8,128)(2,1)S(1)}, f32[16,25...) custom-call(bf16[128,512]{1,0:T(8,128)(2,1)} %refs_0_.1, ...), custom_call_target="tpu_custom_call" | custom-call | tf_op jit(solution)/shard_map/exchange/pallas_call | solution.py:381
  61.2 0.9 %store.1 = (f32[16,256]{1,0:T(8,128)}, f32[16,256]{1,0:T(8,128)}, bf16[16,256]{1,0:T(8,128)(2,1)}, bf16[16,256]{1,0:T(8,128)(2,1)}, f32[16,256]{1,0:T(8,128)}, /...) custom-call(f32[16,256]{1,0:T(8,128)S(1)} %get-tuple-element.24.refs, ...), custom_call_target="tpu_custom_call" | custom-call | tf_op jit(solution)/shard_map/store/pallas_call | solution.py:422

commit v5 on v4

--- a/solution.py
+++ b/solution.py
@@ -11,7 +11,7 @@
 HEAD = 128
 FS = ("fs_0", "fs_1", "fs_2")
 MESH = pl.DeviceIdType.MESH
-SEMS = 22
+SEMS = 27
 TILES = 698
 
 stat_decay = 0.9
@@ -81,7 +81,7 @@
     held, refs = refs[:17], refs[17:]
     x_ref, qg_ref, fg_ref, fp_ref, lb_ref, rq_ref, rf_ref, cq_ref, cf_ref = held[:9]
     (
-    xt, xx, gx, rpack, rin, pmine, pout, pin, gp, rd, ru, sb, rf, gz, gc, o, orv, lp, lin, gram, gin, quarter, colin, sq, sqx, sqsem,
+    xt, xx, gx, rpack, rin, pmine, pout, pin, gp, rd, ru, sb, rf, gz, gc, o, orv, lp, lin, gram, gin, quarter, colin, sq, sqx, sqroom, sums, sqsem,
     room, send, recv, loads,
     ) = refs
     z, x, k, y = (lax.axis_index(n) for n in ("fs_0", "fs_1", "fs_2", "tp"))
@@ -99,9 +99,10 @@
     ]
 
     barrier = pltpu.get_barrier_semaphore()
-    partners = [dict(fs_1=at(x, dx, 4), tp=at(y, dy, 4), fs_2=kk) for dx, dy, kk in plane]
-    partners += [dict(fs_0=zat(n)) for n in (6, -6, 4, -4, 3, -3, 2, -2, 1, -1)]
-    partners += [dict(fs_0=zat(n), fs_2=ko) for n in (1, -1)]
+    partners = [dict(fs_0=zat(n)) for n in (3, -3, 2, -2, 1, -1)]
+    partners += [dict(fs_1=at(x, d, 4)) for d in steps]
+    partners += [dict(tp=at(y, d, 4)) for d in steps]
+    partners += [dict(fs_2=ko)]
     for who in partners:
         pl.semaphore_signal(barrier, inc=1, device_id=who, device_id_type=MESH)
 
@@ -129,8 +130,17 @@
             net.copy(("y", d), xx.at[y, n], xx.at[y, n], tp=at(y, d, 4))
 
     ysend(x)
-    for d in steps:
-        net.copy("g", gx.at[x], gx.at[x], fs_1=at(x, d, 4))
+    halves = (pl.ds(0, 64), pl.ds(64, 64))
+
+    def gcopy(name, n, m, h, d):
+        net.copy(name, gx.at[n, m, h], gx.at[n, m, h], fs_1=at(x, d, 4))
+
+    for i, h in enumerate(halves):
+        gcopy(("gq", i), x, 0, h, 1)
+        gcopy(("gf", i), x, 1, h, -1)
+    for h in halves:
+        gcopy("g", x, 1, h, 1)
+        gcopy("g", x, 0, h, -1)
     for c in load[5:9]:
         c.wait()
     for m, ref in enumerate((rq_ref, rf_ref)):
@@ -173,6 +183,11 @@
             def _():
                 net.copy("s", gp.at[a, q], rd.at[lax.rem(d + 3, 16)], count=False, fs_0=t)
 
+    for i, h in enumerate(halves):
+        net.wait(("gq", i))
+        gcopy("g", at(x, -1, 4), 0, h, 1)
+        net.wait(("gf", i))
+        gcopy("g", at(x, 1, 4), 1, h, -1)
     net.wait("g")
     product(0, y)
     net.wait(("y", 1))
@@ -191,6 +206,7 @@
     net.sent["s"], net.sent["u"] = 6 * 4, 7 * 4
     net.wait("u")
     part = lambda t: pmine[t // 4, lax.rem(t, 4)]
+    net.wait("s")
     for n, e, slots in ((0, 6, (0, 1, 3, 4)), (1, -6, (6, 8, 9))):
         total = part(zat(e))
         for i in slots:
@@ -198,7 +214,6 @@
         sb[n] = total.astype(bf16)
         net.copy("f", sb.at[n], rf.at[2 + 2 * n], fs_0=zat(e))
         net.copy("f", sb.at[n], rf.at[3 + 2 * n], fs_0=zat(2 * e))
-    net.wait("s")
     total = part(z)
     for i in (0, 1, 2, 4, 5, 6):
         total = total + rd[i].astype(f32)
@@ -236,15 +251,15 @@
         for q in range(8):
             o[q // 2, q % 2, i] = block[q * 16 : (q + 1) * 16]
 
-    def osend(h):
+    def osend(group, h):
         orv[k, x, y, h] = o[x, k, h]
         for dx, dy, kk in plane:
             to_x, to_y = at(x, dx, 4), at(y, dy, 4)
-            net.copy("o", o.at[to_x, kk, h], orv.at[k, x, y, h], fs_1=to_x, tp=to_y, fs_2=kk)
+            net.copy(("o", group), o.at[to_x, kk, h], orv.at[k, x, y, h], fs_1=to_x, tp=to_y, fs_2=kk)
 
     outer(0)
     outer(1)
-    osend(pl.ds(0, 2))
+    osend(0, pl.ds(0, 2))
     net.wait(("z", "last"))
     whole = gc[...].reshape(512, 256)
     for h in range(2):
@@ -261,16 +276,17 @@
     sq[0] = jnp.broadcast_to(square, (1, 128))
     outer(2)
     outer(3)
-    for n, (dx, dy, kk) in enumerate(plane):
+    sqx[k, 4 * x + y] = sq[0]
+    for dx, dy, kk in plane:
         pltpu.make_async_remote_copy(
             src_ref=sq.at[0],
-            dst_ref=sqx.at[n],
+            dst_ref=sqx.at[k, 4 * x + y],
             send_sem=sqsem.at[0],
             recv_sem=sqsem.at[1],
             device_id=dict(fs_1=at(x, dx, 4), tp=at(y, dy, 4), fs_2=kk),
             device_id_type=MESH,
         ).start()
-    osend(pl.ds(2, 2))
+    osend(1, pl.ds(2, 2))
     roots = rin[...].reshape(8, 4, 16, 128)
     roots = jnp.concatenate(
         [jnp.concatenate([roots[q, n] for n in range(4)], axis=1) for q in range(8)], axis=0
@@ -305,11 +321,31 @@
             pre[m, h] = dot(high[:, lanes], ref[h]) + dot(low[:, lanes], ref[h])
     for c in load[9:]:
         c.wait()
-    net.wait("o")
+    lane = lax.broadcasted_iota(jnp.int32, (16, 128), 1) // 32
+
+    def gather_rows(group):
+        net.wait(("o", group))
+        for m in range(2):
+            for i in (2 * group, 2 * group + 1):
+                parts = []
+                for n in range(4):
+                    total = orv[m, n, 0, i].astype(f32)
+                    for q in range(1, 4):
+                        total = total + orv[m, n, q, i].astype(f32)
+                    parts.append(total)
+                for e in range(4):
+                    block = parts[0] if e == 0 else pltpu.roll(parts[0], (128 - 32 * e) % 128, 1)
+                    for n in range(1, 4):
+                        turn = (32 * (n - e)) % 128
+                        block = jnp.where(lane == n, pltpu.roll(parts[n], turn, 1) if turn else parts[n], block)
+                    sums[m, i, e] = block
+
+    gather_rows(0)
+    gather_rows(1)
     net.wait("col")
     squares = pltpu.make_async_remote_copy(
-        src_ref=sqx,
-        dst_ref=sqx,
+        src_ref=sqroom,
+        dst_ref=sqroom,
         send_sem=sqsem.at[0],
         recv_sem=sqsem.at[1],
         device_id=dict(fs_2=ko),
@@ -317,35 +353,20 @@
     )
     squares.wait_recv()
     squares.wait_send()
-    same, cross = sq[0], jnp.zeros((1, 128), f32)
-    for n, (dx, dy, kk) in enumerate(plane):
-        if kk is k:
-            same = same + sqx[n]
-        else:
-            cross = cross + sqx[n]
-    lane = lax.broadcasted_iota(jnp.int32, (16, 128), 1) // 32
     for m in range(2):
         master_ref, copy_ref, step_ref, moment_ref, rows_ref, cols_ref = made[m::2]
         weight_old, moment_old, rows_old, cols_old = held[9 + m :: 2]
-        square = jnp.where(k == m, same, cross)
+        square = sqx[m, 0]
+        for n in range(1, 16):
+            square = square + sqx[m, n]
         scale = jnp.sqrt(D * HW / (square + 1.0))
         twice = scale * scale
         by_row = (1.0 - stat_decay) / HW * twice
         by_col = (1.0 - stat_decay) / D * twice
         for i in range(4):
-            sums = []
-            for n in range(4):
-                total = orv[m, n, 0, i].astype(f32)
-                for q in range(1, 4):
-                    total = total + orv[m, n, q, i].astype(f32)
-                sums.append(by_row * total)
             for e in range(4):
-                block = sums[0] if e == 0 else pltpu.roll(sums[0], (128 - 32 * e) % 128, 1)
-                for n in range(1, 4):
-                    turn = (32 * (n - e)) % 128
-                    block = jnp.where(lane == n, pltpu.roll(sums[n], turn, 1) if turn else sums[n], block)
                 lanes = pl.ds(pl.multiple_of(zat(chunks[i][e]) * 128, 128), 128)
-                rows_ref[:, lanes] = stat_decay * rows_old[:, lanes] + block
+                rows_ref[:, lanes] = stat_decay * rows_old[:, lanes] + by_row * sums[m, i, e]
         for h in range(2):
             lanes = slice(h * 128, (h + 1) * 128)
             precond = scale * pre[m, h]
@@ -409,7 +430,9 @@
             s((2, 64, HEAD)),
             s((2, 2, 2, 64, HEAD)),
             s((1, 1, 128), f32),
+            s((2, 16, 1, 128), f32),
             s((31, 1, 128), f32),
+            s((2, 4, 4, 16, 128), f32),
             pltpu.SemaphoreType.DMA((2,)),
             s((TILES, 16, 128)),
             pltpu.SemaphoreType.DMA,

time: 62.3 us -> 59.8 us (0.960)
  Pallas kernels: 61.5 us -> 59 us
    pallas_call x1, Pallas kernels: 60.5 us -> 58.1 us  [on_device(): pl.pallas_call(kernel, out_shape=tuple((pltpu.VMEM(*v) for v in shapes)),...]
where the time goes in v5:
time: 59.8 us; the launch traced here: 59.7 us
  Pallas kernels  59 us (99%)
  between operations  0.66 us (1%)
    pallas_call x1, Pallas kernels, on_device(): pl.pallas_call(kernel, out_shape=tuple((pltpu.VMEM(*v) for v in shapes)),...  58.1 us

profile of v5, /device:TPU:1, one launch (start us, length us, event | category | flops | bytes accessed | tf_op | source)
XLA Modules:
  0.0 59.7 jit_solution(4554479877302532031)
XLA Ops:
  0.7 58.1 %exchange.1 = (f32[16,256]{1,0:T(8,128)S(1)}, f32[16,256]{1,0:T(8,128)S(1)}, bf16[16,256]{1,0:T(8,128)(2,1)S(1)}, bf16[16,256]{1,0:T(8,128)(2,1)S(1)}, f32[16,25...) custom-call(bf16[128,512]{1,0:T(8,128)(2,1)} %refs_0_.1, ...), custom_call_target="tpu_custom_call" | custom-call | tf_op jit(solution)/shard_map/exchange/pallas_call | solution.py:402
  58.7 0.9 %store.1 = (f32[16,256]{1,0:T(8,128)}, f32[16,256]{1,0:T(8,128)}, bf16[16,256]{1,0:T(8,128)(2,1)}, bf16[16,256]{1,0:T(8,128)(2,1)}, f32[16,256]{1,0:T(8,128)}, /...) custom-call(f32[16,256]{1,0:T(8,128)S(1)} %get-tuple-element.24.refs, ...), custom_call_target="tpu_custom_call" | custom-call | tf_op jit(solution)/shard_map/store/pallas_call | solution.py:445

commit v6 on v5

--- a/solution.py
+++ b/solution.py
@@ -81,7 +81,7 @@
     held, refs = refs[:17], refs[17:]
     x_ref, qg_ref, fg_ref, fp_ref, lb_ref, rq_ref, rf_ref, cq_ref, cf_ref = held[:9]
     (
-    xt, xx, gx, rpack, rin, pmine, pout, pin, gp, rd, ru, sb, rf, gz, gc, o, orv, lp, lin, gram, gin, quarter, colin, sq, sqx, sqroom, sums, sqsem,
+    xt, xx, gx, rpack, rin, pmine, pout, pin, gp, rd, ru, sb, rf, gz, gc, o, orv, lp, lin, gram, gin, quarter, colin, sq, sqx, sqroom, sums, sqsem, tokens,
     room, send, recv, loads,
     ) = refs
     z, x, k, y = (lax.axis_index(n) for n in ("fs_0", "fs_1", "fs_2", "tp"))
@@ -99,10 +99,9 @@
     ]
 
     barrier = pltpu.get_barrier_semaphore()
-    partners = [dict(fs_0=zat(n)) for n in (3, -3, 2, -2, 1, -1)]
-    partners += [dict(fs_1=at(x, d, 4)) for d in steps]
+    partners = [dict(fs_1=at(x, d, 4)) for d in steps]
     partners += [dict(tp=at(y, d, 4)) for d in steps]
-    partners += [dict(fs_2=ko)]
+    partners += [dict(fs_0=zat(n)) for n in (1, -1)] + [dict(fs_2=ko)]
     for who in partners:
         pl.semaphore_signal(barrier, inc=1, device_id=who, device_id_type=MESH)
 
@@ -130,6 +129,12 @@
             net.copy(("y", d), xx.at[y, n], xx.at[y, n], tp=at(y, d, 4))
 
     ysend(x)
+
+    def token(n):
+        for e in (1, -1):
+            pl.semaphore_signal(tokens.at[n], inc=1, device_id=dict(fs_0=zat(e)), device_id_type=MESH)
+
+    token(0)
     halves = (pl.ds(0, 64), pl.ds(64, 64))
 
     def gcopy(name, n, m, h, d):
@@ -183,20 +188,23 @@
             def _():
                 net.copy("s", gp.at[a, q], rd.at[lax.rem(d + 3, 16)], count=False, fs_0=t)
 
+    pl.semaphore_wait(tokens.at[0], 2)
+    token(1)
     for i, h in enumerate(halves):
         net.wait(("gq", i))
         gcopy("g", at(x, -1, 4), 0, h, 1)
         net.wait(("gf", i))
         gcopy("g", at(x, 1, 4), 1, h, -1)
+    pl.semaphore_wait(tokens.at[1], 2)
     net.wait("g")
     product(0, y)
     net.wait(("y", 1))
     product(1, ym)
     net.wait(("y", 3))
     product(2, yp)
-    scatter(0, y)
     net.wait(("y", 2))
     product(3, y2)
+    scatter(0, y)
     scatter(1, ym)
     scatter(2, yp)
     scatter(3, y2)
@@ -434,6 +442,7 @@
             s((31, 1, 128), f32),
             s((2, 4, 4, 16, 128), f32),
             pltpu.SemaphoreType.DMA((2,)),
+            pltpu.SemaphoreType.REGULAR((2,)),
             s((TILES, 16, 128)),
             pltpu.SemaphoreType.DMA,
             pltpu.SemaphoreType.DMA((SEMS,)),

time: 59.8 us -> 58.2 us (0.973)
  Pallas kernels: 59 us -> 57.4 us
    pallas_call x1, Pallas kernels: 58.1 us -> 56.5 us  [on_device(): pl.pallas_call(kernel, out_shape=tuple((pltpu.VMEM(*v) for v in shapes)),...]
where the time goes in v6:
time: 58.2 us; the launch traced here: 58.1 us
  Pallas kernels  57.4 us (99%)
  between operations  0.66 us (1%)
    pallas_call x1, Pallas kernels, on_device(): pl.pallas_call(kernel, out_shape=tuple((pltpu.VMEM(*v) for v in shapes)),...  56.5 us

profile of v6, /device:TPU:1, one launch (start us, length us, event | category | flops | bytes accessed | tf_op | source)
XLA Modules:
  0.0 58.1 jit_solution(16064704230835929199)
XLA Ops:
  0.7 56.5 %exchange.1 = (f32[16,256]{1,0:T(8,128)S(1)}, f32[16,256]{1,0:T(8,128)S(1)}, bf16[16,256]{1,0:T(8,128)(2,1)S(1)}, bf16[16,256]{1,0:T(8,128)(2,1)S(1)}, f32[16,25...) custom-call(bf16[128,512]{1,0:T(8,128)(2,1)} %refs_0_.1, ...), custom_call_target="tpu_custom_call" | custom-call | tf_op jit(solution)/shard_map/exchange/pallas_call | solution.py:410
  57.1 0.9 %store.1 = (f32[16,256]{1,0:T(8,128)}, f32[16,256]{1,0:T(8,128)}, bf16[16,256]{1,0:T(8,128)(2,1)}, bf16[16,256]{1,0:T(8,128)(2,1)}, f32[16,256]{1,0:T(8,128)}, /...) custom-call(f32[16,256]{1,0:T(8,128)S(1)} %get-tuple-element.24.refs, ...), custom_call_target="tpu_custom_call" | custom-call | tf_op jit(solution)/shard_map/store/pallas_call | solution.py:454

commit v7 on v6

--- a/solution.py
+++ b/solution.py
@@ -98,6 +98,8 @@
         if (dx, dy) != (0, 0) or kk is ko
     ]
 
+    load = [pltpu.make_async_copy(u, v, loads.at[n]) for n, (u, v) in enumerate(zip(given, held))]
+    load[0].start()
     barrier = pltpu.get_barrier_semaphore()
     partners = [dict(fs_1=at(x, d, 4)) for d in steps]
     partners += [dict(tp=at(y, d, 4)) for d in steps]
@@ -105,8 +107,7 @@
     for who in partners:
         pl.semaphore_signal(barrier, inc=1, device_id=who, device_id_type=MESH)
 
-    load = [pltpu.make_async_copy(u, v, loads.at[n]) for n, (u, v) in enumerate(zip(given, held))]
-    for c in load:
+    for c in load[1:9]:
         c.start()
     load[0].wait()
     for n in range(4):
@@ -135,6 +136,8 @@
             pl.semaphore_signal(tokens.at[n], inc=1, device_id=dict(fs_0=zat(e)), device_id_type=MESH)
 
     token(0)
+    for c in load[9:]:
+        c.start()
     halves = (pl.ds(0, 64), pl.ds(64, 64))
 
     def gcopy(name, n, m, h, d):
@@ -188,15 +191,14 @@
             def _():
                 net.copy("s", gp.at[a, q], rd.at[lax.rem(d + 3, 16)], count=False, fs_0=t)
 
-    pl.semaphore_wait(tokens.at[0], 2)
-    token(1)
     for i, h in enumerate(halves):
         net.wait(("gq", i))
         gcopy("g", at(x, -1, 4), 0, h, 1)
         net.wait(("gf", i))
         gcopy("g", at(x, 1, 4), 1, h, -1)
-    pl.semaphore_wait(tokens.at[1], 2)
     net.wait("g")
+    pl.semaphore_wait(tokens.at[0], 2)
+    token(1)
     product(0, y)
     net.wait(("y", 1))
     product(1, ym)
@@ -204,6 +206,7 @@
     product(2, yp)
     net.wait(("y", 2))
     product(3, y2)
+    pl.semaphore_wait(tokens.at[1], 2)
     scatter(0, y)
     scatter(1, ym)
     scatter(2, yp)

time: 58.2 us -> 57.5 us (0.988)
  Pallas kernels: 57.4 us -> 56.7 us
    pallas_call x1, Pallas kernels: 56.5 us -> 55.7 us  [on_device(): pl.pallas_call(kernel, out_shape=tuple((pltpu.VMEM(*v) for v in shapes)),...]
where the time goes in v7:
time: 57.5 us; the launch traced here: 57.4 us
  Pallas kernels  56.7 us (99%)
  between operations  0.66 us (1%)
    pallas_call x1, Pallas kernels, on_device(): pl.pallas_call(kernel, out_shape=tuple((pltpu.VMEM(*v) for v in shapes)),...  55.7 us

profile of v7, /device:TPU:1, one launch (start us, length us, event | category | flops | bytes accessed | tf_op | source)
XLA Modules:
  0.0 57.4 jit_solution(9496993317570302142)
XLA Ops:
  0.7 55.7 %exchange.1 = (f32[16,256]{1,0:T(8,128)S(1)}, f32[16,256]{1,0:T(8,128)S(1)}, bf16[16,256]{1,0:T(8,128)(2,1)S(1)}, bf16[16,256]{1,0:T(8,128)(2,1)S(1)}, f32[16,25...) custom-call(bf16[128,512]{1,0:T(8,128)(2,1)} %refs_0_.1, ...), custom_call_target="tpu_custom_call" | custom-call | tf_op jit(solution)/shard_map/exchange/pallas_call | solution.py:413
  56.4 0.9 %store.1 = (f32[16,256]{1,0:T(8,128)}, f32[16,256]{1,0:T(8,128)}, bf16[16,256]{1,0:T(8,128)(2,1)}, bf16[16,256]{1,0:T(8,128)(2,1)}, f32[16,256]{1,0:T(8,128)}, /...) custom-call(f32[16,256]{1,0:T(8,128)S(1)} %get-tuple-element.24.refs, ...), custom_call_target="tpu_custom_call" | custom-call | tf_op jit(solution)/shard_map/store/pallas_call | solution.py:457
